TPU v7x, 32 devices: a whole 2x2x4 slice. The times are simulated.
32 devices in a mesh: fs: 4 (over z), tp: 4 (over y, x), rep: 2 (over core).
Axes of the slice: x: 2, y: 2, z: 4, core: 2. Of those that a mesh axis runs over, the one named last changes fastest.
Arguments:
- gate_grads: float32 [2, 5632, 2048], P('rep', 'fs', 'tp'), may hold values from -16 to 16, as said below
- gate_velocity: float32 [5632, 2048], P(('fs', 'rep'), 'tp'), may hold values from -31 to 31, as said below
- gate_weight: float32 [5632, 2048], P(('fs', 'rep'), 'tp'), may hold values from -4 to 4
- up_grads: float32 [2, 5632, 2048], P('rep', 'fs', 'tp'), may hold values from -16 to 16, as said below
- up_velocity: float32 [5632, 2048], P(('fs', 'rep'), 'tp'), may hold values from -31 to 31, as said below
- up_weight: float32 [5632, 2048], P(('fs', 'rep'), 'tp'), may hold values from -4 to 4
- branch_grads: float32 [2, 2048, 1024], P('rep', 'fs', 'tp'), may hold values from -16 to 16, as said below
- branch_velocity: float32 [2048, 1024], P(('fs', 'rep'), 'tp'), may hold values from -31 to 31, as said below
- branch_weight: float32 [2048, 1024], P(('fs', 'rep'), 'tp'), may hold values from -4 to 4
Outputs:
- gate_momentum: float32 [5632, 2048], P(('fs', 'rep'), 'tp')
- gate_updated: float32 [5632, 2048], P(('fs', 'rep'), 'tp')
- up_momentum: float32 [5632, 2048], P(('fs', 'rep'), 'tp')
- up_updated: float32 [5632, 2048], P(('fs', 'rep'), 'tp')
- branch_momentum: float32 [2048, 1024], P(('fs', 'rep'), 'tp')
- branch_updated: float32 [2048, 1024], P(('fs', 'rep'), 'tp')
Inputs may be any that keep to these rules, and one draw needn't show every extreme that they name: `gate_grads`: entries vary in scale over rows and over columns. `up_grads`: entries vary in scale over rows and over columns. `branch_grads`: entries vary in scale over rows and over columns. `gate_velocity`: entries vary in scale over rows and over columns. `up_velocity`: entries vary in scale over rows and over columns. `branch_velocity`: entries vary in scale over rows and over columns.
All inputs are finite; a program needn't handle non-finite values.
Results may differ from a plain program's by a relative error of at most 0.039.
Values may be sent and summed in bfloat16 or wider, within the bound.
A program may use at most 64 MiB of HBM per device.

v0:
```python
import functools
import math

import jax
import jax.numpy as jnp
from jax import lax
from jax.experimental import pallas as pl
from jax.experimental.pallas import tpu as pltpu
from jax.sharding import PartitionSpec as P

MOMENT = 0.95
COEF_ONE = 3.4445
COEF_THREE = -4.775
COEF_FIVE = 2.0315
SAFETY = 2.0
RATE = 0.5
SHRINK = 0.95
ITERS = 3
TILE = 512


def polynomial_kernel(across, tile, column_ref, raw_ref, q_ref, g, s0, s1, s2, s3, c0, c1):
    blocks, height, breadth = raw_ref.shape
    size, width = q_ref.shape
    count = size // tile
    pairs = count * (count + 1) // 2
    here = lax.broadcasted_iota(jnp.int32, (height, breadth), 0)
    there = lax.broadcasted_iota(jnp.int32, (height, breadth), 1)

    def sums(t, carry):
        first, second = carry
        wide = raw_ref[t].astype(jnp.float32)
        shift = lax.rem(t, across) * breadth - t // across * height
        trace = jnp.where(here == there + shift, wide, 0.0)
        return (
            first + jnp.sum(trace, axis=0, keepdims=True),
            second + jnp.sum(wide * wide, axis=0, keepdims=True),
        )

    zero = jnp.zeros((1, breadth), jnp.float32)
    first, second = lax.fori_loop(0, blocks, sums, (zero, zero))
    first = jnp.sum(first, axis=1, keepdims=True)
    second = jnp.sum(second, axis=1, keepdims=True)
    ratio = SAFETY * (second + 1.0) / (first + 1.0)
    inverse, scale = 1.0 / ratio, lax.rsqrt(ratio)

    def normalize(t, carry):
        rows = pl.ds(pl.multiple_of(t // across * height, height), height)
        cols = pl.ds(pl.multiple_of(lax.rem(t, across) * breadth, breadth), breadth)
        g[rows, cols] = (raw_ref[t].astype(jnp.float32) * inverse).astype(jnp.bfloat16)
        return carry

    lax.fori_loop(0, blocks, normalize, 0)

    def quadratic(acc, gram, shift):
        down = lax.broadcasted_iota(jnp.int32, acc.shape, 0)
        over = lax.broadcasted_iota(jnp.int32, acc.shape, 1)
        eye = jnp.where(down == over + shift, COEF_ONE, 0.0)
        return eye + COEF_THREE * gram.astype(jnp.float32) + COEF_FIVE * acc

    def product(left, right, out, poly):
        def step(t, carry):
            i = lax.rem(t, count)
            j = lax.rem(i + t // count, count)
            rows = pl.ds(pl.multiple_of(i * tile, tile), tile)
            cols = pl.ds(pl.multiple_of(j * tile, tile), tile)
            acc = jnp.dot(left[rows, :], right[:, cols], preferred_element_type=jnp.float32)
            if poly:
                acc = quadratic(acc, left[rows, cols], (j - i) * tile)
            value = acc.astype(jnp.bfloat16)
            out[rows, cols] = value

            @pl.when(i != j)
            def _():
                out[cols, rows] = value.T

            return carry

        lax.fori_loop(0, pairs, step, 0)

    column = pl.multiple_of(column_ref[0, 0] * width, width)
    mine = pl.ds(column, width)

    def panel(left, right, out, kind):
        def step(i, carry):
            rows = pl.ds(pl.multiple_of(i * tile, tile), tile)
            acc = jnp.dot(left[rows, :], right[...], preferred_element_type=jnp.float32)
            if kind == "poly":
                acc = quadratic(acc, left[rows, mine], column - i * tile)
            if kind == "scale":
                acc = acc * scale
            out[rows, :] = acc.astype(jnp.bfloat16)
            return carry

        lax.fori_loop(0, count, step, 0)

    product(g, g, s0, True)
    product(g, s0, s1, False)
    product(s1, s0, s2, False)
    product(s2, s2, s1, True)
    product(s2, s1, s3, False)
    product(s3, s1, g, False)
    c1[...] = g[:, mine]
    panel(g, c1, c0, "poly")
    panel(s1, c0, c1, "")
    panel(s0, c1, q_ref, "scale")


def polynomial(blocks, across):
    size = blocks.shape[2] * across
    width = blocks.shape[2]
    tile = min(TILE, size)
    matrix = pltpu.VMEM((size, size), jnp.bfloat16)
    strip = pltpu.VMEM((size, width), jnp.bfloat16)
    return pl.pallas_call(
        functools.partial(polynomial_kernel, across, tile),
        out_shape=jax.ShapeDtypeStruct((size, width), jnp.bfloat16),
        in_specs=[
            pl.BlockSpec(memory_space=pltpu.SMEM),
            pl.BlockSpec(memory_space=pltpu.VMEM),
        ],
        out_specs=pl.BlockSpec(memory_space=pltpu.VMEM),
        scratch_shapes=[matrix] * 5 + [strip] * 2,
        compiler_params=pltpu.CompilerParams(
            vmem_limit_bytes=12 * size * size + 6 * size * width + 8 * 1024 * 1024
        ),
        cost_estimate=pl.CostEstimate(
            flops=10 * size**3, bytes_accessed=3 * size * size, transcendentals=0
        ),
        name=f"polynomial_{size}",
    )(lax.axis_index("tp").astype(jnp.int32).reshape(1, 1), blocks)


def partial_gram(whole, current):
    return lax.dot_general(
        whole, current, (((0,), (0,)), ((), ())), preferred_element_type=jnp.float32
    ).astype(jnp.bfloat16)


def local(nfs, ntp, nrep, *args):
    grads, velocities, weights = args[0::3], args[1::3], args[2::3]
    totals = [
        lax.psum_scatter(g.astype(jnp.bfloat16), "rep", scatter_dimension=1, tiled=True)[0]
        for g in grads
    ]
    moments = [MOMENT * v + t.astype(jnp.float32) for v, t in zip(velocities, totals)]
    starts = [moment.astype(jnp.bfloat16) for moment in moments]
    starts = lax.optimization_barrier(starts)
    wholes = [lax.all_gather(start, "tp", axis=1, tiled=True) for start in starts]
    parts = [partial_gram(whole, start) for whole, start in zip(wholes, starts)]

    shares = nfs * nrep
    size, width = parts[0].shape
    depth, narrow = parts[nrep].shape
    fold = width // narrow
    pair = jnp.stack([part.reshape(nfs, size // nfs, width) for part in parts[:nrep]], axis=1)
    pair = pair.reshape(shares, size // nfs, width)
    third = parts[nrep].reshape(shares, fold, depth // shares // fold, narrow)
    third = jnp.concatenate([third[:, index] for index in range(fold)], axis=2)
    both = jnp.concatenate([pair, third], axis=1)
    share = lax.psum_scatter(
        both.reshape(-1, width), ("fs", "rep"), scatter_dimension=0, tiled=True
    )
    blocks = lax.all_gather(share[: size // nfs], ("fs", "tp"), axis=0, tiled=False)
    tail = share[size // nfs :]
    last = jnp.concatenate(
        [tail[:, index * narrow : (index + 1) * narrow] for index in range(fold)], axis=0
    )
    blocks, last = lax.optimization_barrier((blocks, last))
    gathered = lax.all_gather(last, ("fs", "rep", "tp"), axis=0, tiled=False)
    mine = polynomial(blocks, ntp)
    columns = lax.all_gather(mine, "rep", axis=0, tiled=False)
    factors = [columns[index] for index in range(nrep)]
    factors.append(polynomial(gathered, ntp))

    results = []
    for moment, weight, whole, factor in zip(moments, weights, wholes, factors):
        rows = moment.shape[0] * nfs * nrep
        final = jnp.dot(whole, factor, preferred_element_type=jnp.float32)
        results.append(moment)
        results.append(SHRINK * weight - RATE * math.sqrt(rows) * final)
    return tuple(results)


def solution(mesh):
    sizes = mesh.shape
    split = P(("fs", "rep"), "tp")
    return jax.shard_map(
        functools.partial(local, sizes["fs"], sizes["tp"], sizes["rep"]),
        mesh=mesh,
        in_specs=(P("rep", "fs", "tp"), split, split) * 3,
        out_specs=(split,) * 6,
        check_vma=False,
    )
```

profile of v0, /device:TPU:7, one launch (start us, length us, event | category | flops | bytes accessed | tf_op | source)
XLA Modules:
  0.0 459.2 jit_solution(13336927461155373531)
XLA Ops:
  7.2 0.0 reduce-scatter.9.cloned.1.call-start
  7.2 1.8 convert_element_type.53
  9.0 0.0 reduce-scatter.9.cloned.1.call-update
  9.0 0.0 copy-start.1
  9.0 0.0 reduce-scatter.7.cloned.1.call-start
  9.1 3.2 convert_element_type.49
  12.3 0.0 reduce-scatter.7.cloned.1.call-update
  12.3 0.0 copy-start.7
  12.4 0.0 reduce-scatter.5.cloned.1.call-start
  12.4 0.0 copy-done.1
  12.4 1.3 convert_element_type.45
  13.7 0.0 copy-start.5
  13.7 0.0 reduce-scatter.5.cloned.1.call-update
  13.7 0.0 all-gather.11.cloned.1.call-start
  13.8 6.7 %reduce-scatter.9.cloned.1.call-done = bf16[1,256,256]{2,1,0:T(8,128)(2,1)} async-done(((bf16[1,512,256]{2,1,0:T(8,128)(2,1)}), bf16[1,256,256]{2,1,0:T(8,128)(2,1)}) %reduce-scatter.9.cloned.1.call-update) | async-done | bytes 131088 | tf_op jit(solution)/shard_map/reduce_scatter | solution.py:143
  20.4 0.0 copy-done.7
  20.4 1.6 fusion.15
  22.1 0.0 copy-start.6
  22.1 11.2 %reduce-scatter.7.cloned.1.call-done = bf16[1,704,512]{2,1,0:T(8,128)(2,1)} async-done(((bf16[1,1408,512]{2,1,0:T(8,128)(2,1)}), bf16[1,704,512]{2,1,0:T(8,128)(2,1)}) %reduce-scatter.7.cloned.1.call-update) | async-done | bytes 720912 | tf_op jit(solution)/shard_map/reduce_scatter | solution.py:143
  33.3 0.0 copy-done.5
  33.3 2.7 fusion.16
  36.0 10.3 %reduce-scatter.5.cloned.1.call-done = bf16[1,704,512]{2,1,0:T(8,128)(2,1)} async-done(((bf16[1,1408,512]{2,1,0:T(8,128)(2,1)}), bf16[1,704,512]{2,1,0:T(8,128)(2,1)}) %reduce-scatter.5.cloned.1.call-update) | async-done | bytes 720912 | tf_op jit(solution)/shard_map/reduce_scatter | solution.py:143
  46.3 0.0 copy-done.6
  46.3 2.7 fusion.17
  49.0 0.0 all-gather.11.cloned.1.call-update
  49.0 0.0 all-gather.9.cloned.1.call-start
  49.0 0.5 all-gather.9.cloned.1.call-update
  49.6 0.0 reduce-scatter.11.cloned.1.call-start
  49.6 13.9 %all_gather.29 = bf16[256,1024]{1,0:T(8,128)(2,1)S(1)} all-gather(bf16[256,256]{1,0:T(8,128)(2,1)S(1)} %get-tuple-element.13), channel_id=1, replica_groups=mesh['fs'=4,'tp'=4,'rep'=2] {'tp'}, dimensions={1}, use_global_device_ids=true | all-gather | bytes 655360 | tf_op jit(solution)/shard_map/all_gather | solution.py:149
  63.5 0.4 convolution_convert_fusion.2
  63.9 0.0 copy-start.3
  63.9 29.4 %all-gather.11.cloned.1.call-done = bf16[704,2048]{1,0:T(8,128)(2,1)} async-done(((bf16[704,512]{1,0:T(8,128)(2,1)}), bf16[704,2048]{1,0:T(8,128)(2,1)}) %all-gather.11.cloned.1.call-update) | async-done | bytes 2883600 | tf_op jit(solution)/shard_map/all_gather | solution.py:149
  93.3 0.0 copy-done.2
  93.3 5.0 %convolution_convert_fusion = bf16[2048,512]{1,0:T(8,128)(2,1)} fusion(bf16[704,2048]{1,0:T(8,128)(2,1)} %all-gather.11.cloned.1.call-done, bf16[704,512]{1,0:T(8,128)(2,1)S(1)} %copy-done.2), kind=kOutput, calls=%fused_computation.2 | convolution fusion | flops 1477443584 | bytes 5701632 | tf_op jit(solution)/shard_map/dot_general | solution.py:135
  98.3 38.8 %all-gather.9.cloned.1.call-done = bf16[704,2048]{1,0:T(8,128)(2,1)} async-done(((bf16[704,512]{1,0:T(8,128)(2,1)}), bf16[704,2048]{1,0:T(8,128)(2,1)}) %all-gather.9.cloned.1.call-update) | async-done | bytes 2883600 | tf_op jit(solution)/shard_map/all_gather | solution.py:149
  137.1 0.0 copy-done.3
  137.1 3.8 convolution_convert_fusion.1
  141.0 0.0 copy-done.4
  141.0 0.4 pad_maximum_fusion
  141.4 2.3 maximum_maximum_fusion
  143.7 0.0 reduce-scatter.11.cloned.1.call-update
  143.7 0.0 all-gather.13.cloned.1.call-start
  143.8 54.2 %reduce-scatter.11.cloned.1.call-done = bf16[576,512]{1,0:T(8,128)(2,1)} async-done(((bf16[4608,512]{1,0:T(8,128)(2,1)}), bf16[576,512]{1,0:T(8,128)(2,1)}) %reduce-scatter.11.cloned.1.call-update) | async-done | bytes 589840 | tf_op jit(solution)/shard_map/reduce_scatter | solution.py:161
  198.0 1.9 slice.35
  199.8 0.0 all-gather.13.cloned.1.call-update
  199.8 0.0 all-gather.17.cloned.1.call-start
  199.9 0.8 fusion.18
  200.7 0.6 pad_maximum_fusion.1
  201.3 110.2 %all-gather.13.cloned.1.call-done = bf16[8192,512]{1,0:T(8,128)(2,1)} async-done(((bf16[512,512]{1,0:T(8,128)(2,1)}), bf16[8192,512]{1,0:T(8,128)(2,1)}) %all-gather.13.cloned.1.call-update) | async-done | bytes 8388624 | tf_op jit(solution)/shard_map/all_gather | solution.py:164
  311.5 0.0 all-gather.17.cloned.1.call-update
  311.5 0.2 all-gather.15.cloned.1.call-start
  311.7 110.2 %polynomial_2048.1 = bf16[2048,512]{1,0:T(8,128)(2,1)} custom-call(s32[1,1]{1,0:T(1,128)} %bitcast.3.column_ref, bf16[16,512,512]{2,1,0:T(8,128)(2,1)} %bitcast.48), custom_call_target="tpu_custom_call" | custom-call | flops 85899345920 | bytes 12582912 | tf_op jit(solution)/shard_map/polynomial_2048/pallas_call | solution.py:115
  421.9 0.0 all-gather.15.cloned.1.call-update
  421.9 0.0 all-gather.17.cloned.1.call-done
  422.0 0.0 copy-start
  422.0 1.6 copy-done
  423.6 19.5 %polynomial_1024.1 = bf16[1024,256]{1,0:T(8,128)(2,1)S(1)} custom-call(s32[1,1]{1,0:T(1,128)} %bitcast.3.column_ref, bf16[32,128,256]{2,1,0:T(8,128)(2,1)S(1)} %bitcast.42), custom_call_target="tpu_custom_call" | custom-call | flops 10737418240 | bytes 3145728 | tf_op jit(solution)/shard_map/polynomial_1024/pallas_call | solution.py:115
  443.1 0.0 copy-done.8
  443.1 1.0 fusion.14
  444.1 5.8 %multiply_subtract_fusion.1 = f32[704,512]{1,0:T(8,128)} fusion(f32[704,512]{1,0:T(8,128)} %param.11, bf16[704,2048]{1,0:T(8,128)(2,1)} %all-gather.9.cloned.1.call-done, bf16[4096,512]{1,0:T(8,128)(2,1)} %all-gather.15.cloned.1.call-done), kind=kOutput, calls=%fused_computation.13 | convolution fusion | flops 1477476352 | bytes 7864320 | tf_op jit(solution)/shard_map/dot_general | solution.py:179
  449.9 0.0 copy-done.10
  449.9 0.0 copy-done.9
  449.9 0.0 copy-done.11
  449.9 2.8 multiply_subtract_fusion
  (8 shorter events, 0.0 us)
Async XLA Ops:
  7.2 13.3 %reduce-scatter.9.cloned.1.call-start = ((), (), s32[]{:S(2)}) async-start(), calls=%async_computation.6 | async-start | bytes 393216 | tf_op jit(solution)/shard_map/reduce_scatter | solution.py:143
  9.0 3.4 copy-start.1
  9.0 24.2 %reduce-scatter.7.cloned.1.call-start = ((), (), s32[]{:S(2)}) async-start(), calls=%async_computation.5 | async-start | bytes 2162688 | tf_op jit(solution)/shard_map/reduce_scatter | solution.py:143
  12.3 8.1 %copy-start.7 = (f32[256,256]{1,0:T(8,128)S(1)}, f32[256,256]{1,0:T(8,128)}, u32[]{:S(2)}) copy-start(f32[256,256]{1,0:T(8,128)} %param.16) | copy-start | bytes 786436
  12.4 33.9 %reduce-scatter.5.cloned.1.call-start = ((), (), s32[]{:S(2)}) async-start(), calls=%async_computation.4 | async-start | bytes 2162688 | tf_op jit(solution)/shard_map/reduce_scatter | solution.py:143
  13.7 19.6 %copy-start.5 = (f32[704,512]{1,0:T(8,128)S(1)}, f32[704,512]{1,0:T(8,128)}, u32[]{:S(2)}) copy-start(f32[704,512]{1,0:T(8,128)} %param.13) | copy-start | bytes 4325380
  13.7 79.6 %all-gather.11.cloned.1.call-start = ((), (), s32[]{:S(2)}) async-start(), calls=%async_computation.8 | async-start | bytes 3604480 | tf_op jit(solution)/shard_map/all_gather | solution.py:149
  22.1 24.2 %copy-start.6 = (f32[704,512]{1,0:T(8,128)S(1)}, f32[704,512]{1,0:T(8,128)}, u32[]{:S(2)}) copy-start(f32[704,512]{1,0:T(8,128)} %param.10) | copy-start | bytes 4325380
  49.0 44.4 %copy-start.2 = (bf16[704,512]{1,0:T(8,128)(2,1)S(1)}, bf16[704,512]{1,0:T(8,128)(2,1)}, u32[]{:S(2)}) copy-start(bf16[704,512]{1,0:T(8,128)(2,1)} %get-tuple-element.12) | copy-start | bytes 2162692
  49.0 88.1 %all-gather.9.cloned.1.call-start = ((), (), s32[]{:S(2)}) async-start(), calls=%async_computation.7 | async-start | bytes 3604480 | tf_op jit(solution)/shard_map/all_gather | solution.py:149
  49.6 148.4 %reduce-scatter.11.cloned.1.call-start = ((), (), s32[]{:S(2)}) async-start(), calls=%async_computation.9 | async-start | bytes 5308416 | tf_op jit(solution)/shard_map/reduce_scatter | solution.py:161
  63.9 73.2 %copy-start.3 = (bf16[704,512]{1,0:T(8,128)(2,1)S(1)}, bf16[704,512]{1,0:T(8,128)(2,1)}, u32[]{:S(2)}) copy-start(bf16[704,512]{1,0:T(8,128)(2,1)} %get-tuple-element.11) | copy-start | bytes 2162692
  137.1 3.8 copy-start.4
  143.7 167.8 %all-gather.13.cloned.1.call-start = ((), (), s32[]{:S(2)}) async-start(), calls=%async_computation.10 | async-start | bytes 8912896 | tf_op jit(solution)/shard_map/all_gather | solution.py:164
  199.8 222.1 %all-gather.17.cloned.1.call-start = ((), (), s32[]{:S(2)}) async-start(), calls=%async_computation.12 | async-start | bytes 2162688 | tf_op jit(solution)/shard_map/all_gather | solution.py:170
  311.5 132.6 %all-gather.15.cloned.1.call-start = ((), (), s32[]{:S(2)}) async-start(), calls=%async_computation.11 | async-start | bytes 6291456 | tf_op jit(solution)/shard_map/all_gather | solution.py:172
  422.0 1.6 copy-start
  423.6 19.5 %copy-start.8 = (f32[256,256]{1,0:T(8,128)S(1)}, f32[256,256]{1,0:T(8,128)}, u32[]{:S(2)}) copy-start(f32[256,256]{1,0:T(8,128)} %param.17) | copy-start | bytes 786436
  444.1 5.8 %copy-start.10 = (bf16[704,2048]{1,0:T(8,128)(2,1)S(1)}, bf16[704,2048]{1,0:T(8,128)(2,1)}, u32[]{:S(2)}) copy-start(bf16[704,2048]{1,0:T(8,128)(2,1)} %all-gather.11.cloned.1.call-done) | copy-start | bytes 8650756
  444.1 5.8 %copy-start.9 = (bf16[4096,512]{1,0:T(8,128)(2,1)S(1)}, bf16[4096,512]{1,0:T(8,128)(2,1)}, u32[]{:S(2)}) copy-start(bf16[4096,512]{1,0:T(8,128)(2,1)} %all-gather.15.cloned.1.call-done) | copy-start | bytes 12582916
  444.1 5.8 %copy-start.11 = (f32[704,512]{1,0:T(8,128)S(1)}, f32[704,512]{1,0:T(8,128)}, u32[]{:S(2)}) copy-start(f32[704,512]{1,0:T(8,128)} %param.14) | copy-start | bytes 4325380
Sparse Core Ops, SparseCore 0:
  10.8 9.6 reduce-scatter.8
  23.3 9.9 reduce-scatter.6
  36.1 10.1 reduce-scatter.4
  49.1 44.1 all-gather.10
  95.6 41.5 all-gather.8
  143.8 54.0 reduce-scatter.10
  201.3 110.1 all-gather.12
  314.9 56.3 all-gather.16
  422.1 15.0 all-gather.14
where the time goes:
time: 464 us; the launch traced here: 459 us
  waiting for transfers between devices  261 us (56%)
  Pallas kernels  130 us (28%)
  matrix products  18.7 us (4%)
  other arithmetic  16.7 us (4%)
  between operations  14 us (3%)
  blocking collectives  13.9 us (3%)
    pallas_call x2, Pallas kernels, polynomial(): pl.pallas_call(functools.partial(polynomial_kernel, across, tile), out_sh...  130 us
    all_gather x1, waiting for transfers between devices, local(): lax.all_gather(share[:size // nfs], ('fs', 'tp'), axis=0, tiled=False)  110 us
    all_gather x2, waiting for transfers between devices, local(): lax.all_gather(start, 'tp', axis=1, tiled=True)  68.2 us
    reduce_scatter x1, waiting for transfers between devices, local(): lax.psum_scatter(both.reshape(-1, width), ('fs', 'rep'), scatter_dimensio...  54.2 us
    reduce_scatter x3, waiting for transfers between devices, local(): lax.psum_scatter(g.astype(jnp.bfloat16), 'rep', scatter_dimension=1, tile...  28.1 us
    all_gather x1, blocking collectives, local(): lax.all_gather(start, 'tp', axis=1, tiled=True)  13.9 us
    dot_general x3, matrix products, local(): final = jnp.dot(whole, factor, preferred_element_type=jnp.float32)  9.57 us
  transfers between devices with their start and end apart: 9, of which 7 were waited for; matrix products, arithmetic and copies ran while one was open for 4% of the time, Pallas kernels for 28%

commit v1 on v0

v1 whole, which is shorter than its diff:
```python
import functools
import math

import jax
import jax.numpy as jnp
from jax import lax
from jax.experimental import pallas as pl
from jax.experimental.pallas import tpu as pltpu
from jax.sharding import PartitionSpec as P

MOMENT = 0.95
COEF_ONE = 3.4445
COEF_THREE = -4.775
COEF_FIVE = 2.0315
SAFETY = 2.0
RATE = 0.5
SHRINK = 0.95
STEP = 64
CHUNK = 176
GRANT = 67043328
F32 = jnp.float32
BF16 = jnp.bfloat16


def at(start, size, unit):
    return pl.ds(pl.multiple_of(start, unit), size)


def fit(rows, most):
    return max(n for n in range(16, most + 1, 16) if rows % n == 0)


def rows_loop(rows, most, body):
    step = fit(rows, most)

    def run(i, carry):
        body(at(i * step, step, step))
        return carry

    lax.fori_loop(0, rows // step, run, 0)


def kernel(nfs, ntp, *refs):
    (gg, gv, gw, ug, uv, uw, bg, bv, bw, gm, gu, um, uu, bm, bu) = refs[:15]
    (s, sb, vel, velb, gs, gsb, go, gob) = refs[15:23]
    (psend, part, prcv, rin, cross, tot, b0, b1, b2, gb) = refs[23:33]
    (c0, c1, c2, qs, qt, qtb, sums) = refs[33:40]
    (loc, rep_s, rep_r, ring_s, ring_r, half_s, half_r, in_s, in_r, mid_r) = refs[40:50]
    (out_s, out_r, ag_s, ag_r, dd_s, dd_r, gd_s, gd_r, pr_s, pr_r, q_s, q_r) = refs[50:62]

    height, size = s.shape[1:]
    width = size // ntp
    half = width // 2
    low, small = sb.shape
    thin = small // ntp
    count = 4
    tile = size // count

    f, t, r = lax.axis_index("fs"), lax.axis_index("tp"), lax.axis_index("rep")

    def turn(v):
        return v + v // 2 * (5 - 2 * v)

    p = turn(t)
    side = t % 2
    other = 1 - r
    peers = [turn((p + d) % ntp) for d in range(ntp)]
    across, beside, diagonal = t + 1 - 2 * side, (t + 2) % ntp, None
    diagonal = (across + 2) % ntp
    first_end, last_end = f == 0, f == nfs - 1
    is_end = jnp.logical_or(first_end, last_end)
    middle = nfs // 2
    is_mid = jnp.logical_or(f == middle - 1, f == middle)
    inward = jnp.where(f < middle, f + 1, f - 1)
    outward = jnp.where(f < middle, f - 1, f + 1)
    mate = {"rep": other}

    def send(src, dst, ssem, rsem, device):
        copy = pltpu.make_async_remote_copy(
            src_ref=src,
            dst_ref=dst,
            send_sem=ssem,
            recv_sem=rsem,
            device_id=device,
            device_id_type=pl.DeviceIdType.MESH,
        )
        return copy

    def arrived(dst, rsem):
        send(dst, dst, rsem, rsem, mate).wait_recv()

    def left(src, ssem):
        send(src, src, ssem, ssem, mate).wait_send()

    barrier = pltpu.get_barrier_semaphore()

    def greet(device):
        pl.semaphore_signal(
            barrier, inc=1, device_id=device, device_id_type=pl.DeviceIdType.MESH
        )

    grads, velocities, weights = (gg, ug, bg), (gv, uv, bv), (gw, uw, bw)
    outs_m, outs_u = (gm, um, bm), (gu, uu, bu)
    extents = ((height, width), (height, width), (low, thin))
    sent32 = (gs.at[0], gs.at[1], gsb)
    own32 = (go.at[0], go.at[1], gob)
    speed = (vel.at[0], vel.at[1], velb)
    txs = tuple(b1.at[:n, m * width : m * width + c] for m, (n, c) in enumerate(extents))
    rxs = tuple(b2.at[:n, m * width : m * width + c] for m, (n, c) in enumerate(extents))

    def local(src, dst, index):
        return pltpu.make_async_copy(src, dst, loc.at[index])

    loads = []
    for m in range(3):
        n = extents[m][0]
        loads.append(
            (
                local(grads[m].at[0, at(other * n, n, n)], sent32[m], m),
                local(grads[m].at[0, at(r * n, n, n)], own32[m], 3 + m),
                local(velocities[m], speed[m], 6 + m),
            )
        )
    for m in range(3):
        loads[m][0].start()
    for m in range(3):
        loads[m][1].start()
        loads[m][2].start()

    greet(mate)
    for d in range(1, ntp):
        greet({"tp": peers[d]})
    pl.when(f > 0)(lambda: greet({"fs": f - 1}))
    pl.when(f < nfs - 1)(lambda: greet({"fs": f + 1}))
    pl.semaphore_wait(barrier, ntp + jnp.minimum(f, 1) + jnp.minimum(nfs - 1 - f, 1))

    for m in range(3):
        loads[m][0].wait()

        def narrow(rows, m=m):
            txs[m][rows, :] = sent32[m][rows, :].astype(BF16)

        rows_loop(extents[m][0], STEP, narrow)
        send(txs[m], rxs[m], rep_s.at[m], rep_r.at[m], mate).start()

    mine = at(t * width, width, width)
    mine_b = at(t * thin, thin, thin)

    def ring(m, d):
        src = s.at[m, :, mine]
        send(src, src, ring_s.at[m, d], ring_r.at[m, d], {"tp": peers[d]}).start()

    def ring_b(d):
        src = sb.at[:, mine_b]
        send(src, src, ring_s.at[2, d], ring_r.at[2, d], {"tp": peers[d]}).start()

    def ring_in(m, d):
        spot = s.at[m, :, at(peers[ntp - d] * width, width, width)]
        arrived(spot, ring_r.at[m, d])

    def momentum(m):
        loads[m][1].wait()
        loads[m][2].wait()
        arrived(rxs[m], rep_r.at[m])

        def add(rows):
            total = own32[m][rows, :] + rxs[m][rows, :].astype(F32)
            value = MOMENT * speed[m][rows, :] + total
            speed[m][rows, :] = value
            if m < 2:
                s[m, rows, mine] = value.astype(BF16)
            else:
                sb[rows, mine_b] = value.astype(BF16)

        rows_loop(extents[m][0], STEP, add)
        local(speed[m], outs_m[m], 9 + m).start()

    def exchange(b, i, make):
        psend[b] = make(other)
        send(psend.at[b], prcv.at[b], half_s.at[i], half_r.at[i], mate).start()
        part[b] = make(r)

    def gram(slot, m, a, b):
        lo, hi = jnp.minimum(a, b), jnp.maximum(a, b)

        def make(h):
            return lax.dot_general(
                s[m, :, at(lo * width + h * half, half, half)],
                s[m, :, at(hi * width, width, width)],
                (((0,), (0,)), ((), ())),
                preferred_element_type=F32,
            ).astype(BF16)

        exchange(slot, slot, make)

    def add_into(b, ref):
        def add(rows):
            value = part[b, rows, :].astype(F32) + ref[rows, :].astype(F32)
            part[b, rows, :] = value.astype(BF16)

        rows_loop(half, STEP, add)

    def to_inner(b, i):
        send(part.at[b], rin.at[b], in_s.at[i], in_r.at[i], {"fs": inward}).start()

    def to_outer(b, i):
        send(tot.at[b], tot.at[b], out_s.at[i], out_r.at[i], {"fs": outward}).start()

    def chain_a(b, i):
        arrived(prcv.at[b], half_r.at[i])
        add_into(b, prcv.at[b])
        pl.when(jnp.logical_and(is_end, jnp.logical_not(is_mid)))(lambda: to_inner(b, i))

    def chain_b(b, i):
        @pl.when(jnp.logical_not(is_end))
        def _():
            arrived(rin.at[b], in_r.at[i])
            add_into(b, rin.at[b])
            pl.when(jnp.logical_not(is_mid))(lambda: to_inner(b, i))

        @pl.when(is_mid)
        def _():
            send(part.at[b], cross.at[i], in_s.at[i], mid_r.at[i], {"fs": inward}).start()

    def chain_c(b, i):
        @pl.when(is_mid)
        def _():
            arrived(cross.at[i], mid_r.at[i])

            def add(rows):
                value = part[b, rows, :].astype(F32) + cross[i, rows, :].astype(F32)
                tot[b, rows, :] = value.astype(BF16)

            rows_loop(half, STEP, add)
            pl.when(jnp.logical_not(is_end))(lambda: to_outer(b, i))

    def chain_d(b, i):
        @pl.when(jnp.logical_not(is_mid))
        def _():
            arrived(tot.at[b], out_r.at[i])
            pl.when(jnp.logical_not(is_end))(lambda: to_outer(b, i))

    def chain_end(b, i):
        left(psend.at[b], half_s.at[i])
        left(part.at[b], in_s.at[i])
        pl.when(jnp.logical_not(is_end))(lambda: left(tot.at[b], out_s.at[i]))

    def place(q, kind, matrix):
        a = turn(q)
        b = {
            0: a,
            1: turn((q + ntp - 1 + 2 * matrix) % ntp),
            2: turn((q + ntp // 2) % ntp),
        }[kind]
        return jnp.minimum(a, b), jnp.maximum(a, b)

    def spot(q, kind, matrix, h):
        i, j = place(q, kind, matrix)
        return b0.at[at(i * width + h * half, half, half), at(j * width, width, width)]

    kinds = (0, 1, 2, 0, 1, 0, 1, 2, 0, 1)
    owners = [p] * 3 + [turn(across)] * 2 + [turn(beside)] * 3 + [turn(diagonal)] * 2

    def gather_own(slot, kind, matrix):
        here = spot(p, kind, matrix, r)
        i, j = place(p, kind, matrix)

        def copy(rows):
            start = i * width + r * half
            b0[at(start + rows.start, STEP, STEP), at(j * width, width, width)] = tot[
                slot, rows, :
            ]

        rows_loop(half, STEP, copy)
        send(
            tot.at[slot], here, ag_s.at[slot, 0], ag_r.at[5 + kind], {"tp": beside}
        ).start()
        send(tot.at[slot], here, dd_s.at[kind], dd_r.at[kind], mate).start()

    def gather_far(slot, kind, matrix):
        here = spot(p, kind, matrix, r)
        send(
            tot.at[slot], here, ag_s.at[slot, 0], ag_r.at[3 + kind], {"tp": across}
        ).start()
        send(
            tot.at[slot], here, ag_s.at[slot, 1], ag_r.at[8 + kind], {"tp": diagonal}
        ).start()

    def gather(slot):
        if slot == 4:
            gather_own(slot, 2, side)
            return
        matrix, kind = slot // 2, slot % 2
        pl.when(side == matrix)(lambda: gather_own(slot, kind, matrix))
        pl.when(side != matrix)(lambda: gather_far(slot, kind, matrix))

    momentum(0)
    ring(0, 1)
    momentum(1)
    ring(1, ntp - 1)
    ring(1 - side, 2)
    gram(0, 0, t, t)
    gram(2, 1, t, t)
    momentum(2)
    chain_a(0, 0)
    chain_a(2, 2)
    chain_b(0, 0)
    chain_b(2, 2)
    ring_in(0, 1)
    gram(1, 0, peers[ntp - 1], t)
    ring_in(1, ntp - 1)
    gram(3, 1, peers[1], t)
    chain_a(1, 1)
    chain_a(3, 3)
    chain_c(0, 0)
    chain_c(2, 2)
    chain_b(1, 1)
    chain_b(3, 3)
    chain_d(0, 0)
    gather(0)
    chain_d(2, 2)
    gather(2)
    ring_in(side, 2)
    gram(4, side, peers[2], t)
    chain_a(4, 4)
    chain_c(1, 1)
    chain_c(3, 3)
    chain_b(4, 4)
    chain_d(1, 1)
    gather(1)
    chain_d(3, 3)
    gather(3)
    chain_c(4, 4)
    chain_d(4, 4)
    gather(4)

    for m in range(3):
        left(txs[m], rep_s.at[m])
    for e in (3, 5, 8, 4, 6, 9, 7):
        here = spot(owners[e], kinds[e], side, r)
        arrived(here, ag_r.at[e])
        send(here, here, dd_s.at[e], dd_r.at[e], mate).start()

    sums[...] = jnp.zeros_like(sums)

    def fold(value):
        return jnp.sum(value.reshape(-1, 8, value.shape[1]), axis=0)

    def survey(ref, i, j, diag, span):
        def add(rows):
            wide = ref[at(i + rows.start, STEP, STEP), at(j, span, span)].astype(F32)
            weight = 1.0 if diag else 2.0
            sums[1, :, :span] += weight * fold(wide * wide)
            if diag:
                down = lax.broadcasted_iota(jnp.int32, wide.shape, 0) + rows.start
                over = lax.broadcasted_iota(jnp.int32, wide.shape, 1)
                sums[0, :, :span] += fold(jnp.where(down == over, wide, 0.0))

        rows_loop(span, STEP, add)

    def scales():
        first = jnp.sum(jnp.sum(sums[0], axis=0, keepdims=True), axis=1, keepdims=True)
        second = jnp.sum(jnp.sum(sums[1], axis=0, keepdims=True), axis=1, keepdims=True)
        ratio = SAFETY * (second + 1.0) / (first + 1.0)
        return 1.0 / ratio, lax.rsqrt(ratio)

    for e in range(10):
        arrived(spot(owners[e], kinds[e], side, other), dd_r.at[e])
        i, j = place(owners[e], kinds[e], side)
        survey(b0, i * width, j * width, kinds[e] == 0, width)
        if kinds[e] != 0:
            b0[at(j * width, width, width), at(i * width, width, width)] = b0[
                at(i * width, width, width), at(j * width, width, width)
            ].T

    for slot in range(5):
        left(tot.at[slot], ag_s.at[slot, 0])
        if slot < 4:
            pl.when(side != slot // 2)(lambda slot=slot: left(tot.at[slot], ag_s.at[slot, 1]))
        chain_end(slot, slot)
    for e in range(10):
        left(tot.at[0], dd_s.at[e])
    ring(0, ntp - 1)
    ring(1, 1)
    ring(side, 2)
    for d in range(1, ntp):
        ring_b(d)
    for m in range(3):
        local(speed[m], outs_m[m], 9 + m).wait()
        local(weights[m], speed[m], 12 + m).start()

    inverse, scale = scales()

    def eye(shape, shift):
        down = lax.broadcasted_iota(jnp.int32, shape, 0)
        over = lax.broadcasted_iota(jnp.int32, shape, 1)
        return jnp.where(down == over + shift, COEF_ONE, 0.0)

    def product(index, lhs, rhs, out, finish):
        def where(k, who):
            third, fourth = k // 3, k // 4
            i, j = third - fourth, k - 2 * third + fourth
            i, j = (
                i + who * (3 - j + fourth - i),
                j + who * (3 - i - fourth - j),
            )
            return i, j

        def step(k, carry):
            i, j = where(k, r)
            rows, cols = at(i * tile, tile, tile), at(j * tile, tile, tile)
            acc = jnp.dot(lhs[rows, :], rhs[:, cols], preferred_element_type=F32)
            value = finish(acc, lhs, rows, cols, (j - i) * tile).astype(BF16)
            out[rows, cols] = value
            here = out.at[rows, cols]
            send(here, here, pr_s.at[index, k], pr_r.at[index, k], mate).start()

            @pl.when(i != j)
            def _():
                out[cols, rows] = value.T

            return carry

        lax.fori_loop(0, 5, step, 0)

        def take(k, carry):
            i, j = where(k, other)
            rows, cols = at(i * tile, tile, tile), at(j * tile, tile, tile)
            here = out.at[rows, cols]
            arrived(here, pr_r.at[index, k])

            @pl.when(i != j)
            def _():
                out[cols, rows] = out[rows, cols].T

            left(here, pr_s.at[index, k])
            return carry

        lax.fori_loop(0, 5, take, 0)

    def poly_one(inv):
        def finish(acc, lhs, rows, cols, shift):
            gram_part = lhs[rows, cols].astype(F32) * inv
            return eye(acc.shape, shift) + COEF_THREE * gram_part + COEF_FIVE * (acc * inv * inv)

        return finish

    def times(inv):
        return lambda acc, lhs, rows, cols, shift: acc * inv

    def plain(acc, lhs, rows, cols, shift):
        return acc

    def poly_two(acc, lhs, rows, cols, shift):
        return eye(acc.shape, shift) + COEF_THREE * lhs[rows, cols].astype(F32) + COEF_FIVE * acc

    product(0, b0, b0, b1, poly_one(inverse))

    for d in range(1, ntp):
        arrived(sb.at[:, at(peers[ntp - d] * thin, thin, thin)], ring_r.at[2, d])
    deep, wide_b = small // 2 // half, small // width
    blocks = deep * wide_b
    for b in range(blocks):
        def make(h, b=b):
            return lax.dot_general(
                sb[:, at(h * (small // 2) + b // wide_b * half, half, half)],
                sb[:, b % wide_b * width : (b % wide_b + 1) * width],
                (((0,), (0,)), ((), ())),
                preferred_element_type=F32,
            ).astype(BF16)

        exchange(b, 5 + b, make)
    product(1, b0, b1, b2, times(inverse))
    for b in range(blocks):
        chain_a(b, 5 + b)
    product(2, b2, b1, b0, plain)
    for b in range(blocks):
        chain_b(b, 5 + b)
    product(3, b0, b0, b2, poly_two)
    for b in range(blocks):
        chain_c(b, 5 + b)

    def panel(lhs, rhs, out, span, finish):
        def step(j, carry):
            cols = at(j * tile, tile, tile)
            acc = jnp.dot(lhs(), rhs(cols), preferred_element_type=F32)
            out(cols, finish(acc, cols).astype(BF16))
            return carry

        lax.fori_loop(0, span // tile, step, 0)

    def same(acc, cols):
        return acc

    def factor(begin, g2, p1, p2, span, scaling, out):
        def buf(ref):
            return lambda: ref[:, :span]

        def put(ref):
            def write(cols, value):
                ref[:, cols] = value

            return write

        def cubic(acc, cols):
            shift = cols.start - begin
            return (
                eye(acc.shape, shift)
                + COEF_THREE * c1[:, cols].astype(F32)
                + COEF_FIVE * acc
            )

        panel(lambda: p2(at(begin, half, half), None), lambda c: p2(None, c), put(c0), span, same)
        panel(buf(c0), lambda c: g2(None, c), put(c1), span, same)
        panel(buf(c1), lambda c: g2(None, c), put(c2), span, same)
        panel(buf(c2), lambda c: p2(None, c), put(c0), span, same)
        panel(buf(c0), lambda c: p2(None, c), put(c2), span, cubic)
        panel(buf(c2), lambda c: p2(None, c), put(c0), span, same)
        panel(buf(c0), lambda c: p1(None, c), out, span, lambda acc, cols: acc * scaling)

    def view(ref, top, span):
        def read(rows, cols):
            if rows is None:
                return ref[top : top + span, cols]
            return ref[at(top + rows.start, half, half), :span]

        return read

    big = (view(b0, 0, size), view(b1, 0, size), view(b2, 0, size))

    def put_qs(cols, value):
        qs[:, cols] = value

    def put_qt(cols, value):
        qt[side, at(r * half, half, half), cols] = value

    def put_qb(cols, value):
        qtb[:, cols] = value

    factor(across * width + r * half, *big, size, scale, put_qs)
    landing = qt.at[side, at(r * half, half, half)]
    send(qs, landing, q_s.at[0], q_r.at[0], {"tp": across}).start()
    for b in range(blocks):
        chain_d(b, 5 + b)
        a, c = b // wide_b, b % wide_b
        start = r * (small // 2) + a * half
        here = gb.at[at(start, half, half), c * width : (c + 1) * width]

        def copy(rows, b=b, start=start, c=c):
            gb[at(start + rows.start, STEP, STEP), c * width : (c + 1) * width] = tot[b, rows, :]

        rows_loop(half, STEP, copy)
        send(tot.at[b], here, gd_s.at[b], gd_r.at[b], mate).start()
    factor(t * width + r * half, *big, size, scale, put_qt)
    send(landing, landing, q_s.at[1], q_r.at[1], mate).start()

    for b in range(blocks):
        a, c = b // wide_b, b % wide_b
        start = other * (small // 2) + a * half
        arrived(gb.at[at(start, half, half), c * width : (c + 1) * width], gd_r.at[b])
    sums[...] = jnp.zeros_like(sums)
    for i in range(0, small, width):
        for j in range(0, small, width):
            if i == j:
                survey(gb, i, j, True, width)
            if i < j:
                survey(gb, i, j, False, width)
    inverse_b, scale_b = scales()

    def square(lhs, rhs, out, finish):
        def step(n, carry):
            i, j = n // (small // tile), n % (small // tile)
            rows, cols = at(i * tile, tile, tile), at(j * tile, tile, tile)
            acc = jnp.dot(lhs[rows, :small], rhs[:small, cols], preferred_element_type=F32)
            out[rows, cols] = finish(acc, lhs, rows, cols, (j - i) * tile).astype(BF16)
            return carry

        lax.fori_loop(0, (small // tile) ** 2, step, 0)

    square(gb, gb, b1, poly_one(inverse_b))
    square(gb, b1, b2, times(inverse_b))
    square(b2, b1, b0, plain)
    square(b0, b0, b2, poly_two)
    tiny = (view(b0, 0, small), view(b1, 0, small), view(b2, 0, small))
    factor(t * thin, *tiny, small, scale_b, put_qb)

    def update(m, lhs, rhs, rate, ref, rows_of, step):
        def body(rows):
            acc = lax.dot_general(
                lhs(rows), rhs(), (((1,), (1,)), ((), ())), preferred_element_type=F32
            )
            ref(rows, acc, rate)

        rows_loop(rows_of, step, body)

    def put_big(m):
        def write(rows, acc, rate):
            vel[m, rows, :] = SHRINK * vel[m, rows, :] - rate * acc

        return write

    def put_small(rows, acc, rate):
        velb[rows, :] = SHRINK * velb[rows, :] - rate * acc

    rate = RATE * math.sqrt(height * nfs * 2)
    rate_b = RATE * math.sqrt(low * nfs * 2)

    def finish_big(m):
        update(m, lambda rows: s[m, rows, :], lambda: qt[m], rate, put_big(m), height, CHUNK)

        @pl.when(m == 0)
        def _():
            local(speed[0], gu, 15).start()

        @pl.when(m == 1)
        def _():
            local(speed[1], uu, 16).start()

    for m in range(3):
        local(weights[m], speed[m], 12 + m).wait()
    update(2, lambda rows: sb[rows, :], lambda: qtb[...], rate_b, put_small, low, CHUNK)
    local(velb, bu, 17).start()
    ring_in(0, ntp - 1)
    ring_in(1, 1)
    ring_in(1 - side, 2)
    arrived(qt.at[side, at(other * half, half, half)], q_r.at[1])
    finish_big(side)
    far = qt.at[1 - side, at(r * half, half, half)]
    arrived(far, q_r.at[0])
    send(far, far, q_s.at[2], q_r.at[2], mate).start()
    arrived(qt.at[1 - side, at(other * half, half, half)], q_r.at[2])
    finish_big(1 - side)

    for m in range(3):
        for d in range(1, ntp):
            block = s.at[m, :, mine] if m < 2 else sb.at[:, mine_b]
            left(block, ring_s.at[m, d])
    for b in range(blocks):
        chain_end(b, 5 + b)
        left(tot.at[b], gd_s.at[b])
    left(qs, q_s.at[0])
    left(landing, q_s.at[1])
    left(far, q_s.at[2])
    local(speed[0], gu, 15).wait()
    local(speed[1], uu, 16).wait()
    local(velb, bu, 17).wait()


def local_part(nfs, ntp, *args):
    height, width = args[1].shape
    low, thin = args[7].shape
    size, small = width * ntp, thin * ntp
    half = width // 2
    blocks = small // 2 // half * (small // width)
    vmem = pltpu.VMEM
    dma = pltpu.SemaphoreType.DMA
    scratch = [
        vmem((2, height, size), BF16),
        vmem((low, small), BF16),
        vmem((2, height, width), F32),
        vmem((low, thin), F32),
        vmem((2, height, width), F32),
        vmem((low, thin), F32),
        vmem((2, height, width), F32),
        vmem((low, thin), F32),
    ]
    scratch += [vmem((5, half, width), BF16)] * 4
    scratch += [vmem((5 + blocks, half, width), BF16), vmem((5, half, width), BF16)]
    scratch += [vmem((size, size), BF16)] * 3 + [vmem((small, small), BF16)]
    scratch += [vmem((half, size), BF16)] * 4
    scratch += [vmem((2, width, size), BF16), vmem((thin, small), BF16), vmem((2, 8, width), F32)]
    slots = dma((5 + blocks,))
    scratch += [dma((18,)), dma((3,)), dma((3,)), dma((3, ntp)), dma((3, ntp))]
    scratch += [slots] * 7
    scratch += [dma((5, 2)), dma((10,)), dma((10,)), dma((10,)), dma((blocks,)), dma((blocks,))]
    scratch += [dma((4, 5)), dma((4, 5)), dma((3,)), dma((3,))]
    outs = []
    for i in range(3):
        outs += [jax.ShapeDtypeStruct(args[3 * i + 1].shape, F32)] * 2
    return pl.pallas_call(
        functools.partial(kernel, nfs, ntp),
        out_shape=tuple(outs),
        in_specs=[pl.BlockSpec(memory_space=pl.ANY)] * 9,
        out_specs=tuple([pl.BlockSpec(memory_space=pl.ANY)] * 6),
        scratch_shapes=scratch,
        compiler_params=pltpu.CompilerParams(
            collective_id=0, has_side_effects=True, vmem_limit_bytes=GRANT
        ),
        name="orthogonal",
    )(*args)


def solution(mesh):
    sizes = mesh.shape
    split = P(("fs", "rep"), "tp")
    return jax.shard_map(
        functools.partial(local_part, sizes["fs"], sizes["tp"]),
        mesh=mesh,
        in_specs=(P("rep", "fs", "tp"), split, split) * 3,
        out_specs=(split,) * 6,
        check_vma=False,
    )
```

time: 464 us -> 246 us (0.53)
  waiting for transfers between devices: 261 us -> 0 us
  Pallas kernels: 130 us -> 235 us
  matrix products: 18.7 us -> 0 us
  other arithmetic: 16.7 us -> 0 us
  blocking collectives: 13.9 us -> 0 us
  between operations: 14 us -> 0.66 us
  local copies, waits for them, and re-layouts: 4.32 us -> 8.96 us
    all_gather x5 -> x0, waiting for transfers between devices: 178 us -> none  [the longest x1 110 us: local(): lax.all_gather(share[:size // nfs], ('fs', 'tp'), axis=0, tiled=False)]
    pallas_call x2 -> x1, Pallas kernels: 130 us -> 235 us  [local_part(): pl.pallas_call(functools.partial(kernel, nfs, ntp), out_shape=tuple(outs)...]
    reduce_scatter x4 -> x0, waiting for transfers between devices: 82.3 us -> none  [the longest x1 54.2 us: local(): lax.psum_scatter(both.reshape(-1, width), ('fs', 'rep'), scatter_dimensio...]
    dot_general x6 -> x0, matrix products: 18.7 us -> none  [the longest x3 9.57 us: local(): final = jnp.dot(whole, factor, preferred_element_type=jnp.float32)]
    all_gather x1 -> x0, blocking collectives: 13.9 us -> none  [local(): lax.all_gather(start, 'tp', axis=1, tiled=True)]
    convert_element_type x6 -> x0, other arithmetic: 13.4 us -> none  [the longest x3 7.06 us: local(): starts = [moment.astype(jnp.bfloat16) for moment in moments]]
    unnamed x24 -> x16, local copies, waits for them, and re-layouts: 1.63 us -> 8.96 us
  transfers between devices with their start and end apart: 9 -> 0, of which waited for: 7 -> 0; matrix products, arithmetic and copies ran while one was open for 4% -> 0% of each run, Pallas kernels for 28% -> 0%
where the time goes in v1:
time: 246 us; the launch traced here: 244 us
  Pallas kernels  235 us (96%)
  local copies, waits for them, and re-layouts  8.96 us (4%)
    pallas_call x1, Pallas kernels, local_part(): pl.pallas_call(functools.partial(kernel, nfs, ntp), out_shape=tuple(outs)...  235 us
    unnamed x16, local copies, waits for them, and re-layouts  8.96 us

profile of v1, /device:TPU:7, one launch (start us, length us, event | category | flops | bytes accessed | tf_op | source)
XLA Modules:
  0.0 244.3 jit_solution(2878071183375151222)
XLA Ops:
  0.6 234.7 %orthogonal.1 = (f32[704,512]{1,0:T(8,128)}, f32[704,512]{1,0:T(8,128)}, f32[704,512]{1,0:T(8,128)}, f32[704,512]{1,0:T(8,128)}, f32[256,256]{1,0:T(8,128)}, /*index=5*/f32[256,256]{1,0:T(8,128)}) custom-call(f32[1,1408,512]{2,1,0:T(8,128)} %refs_0_.1, f32[704,512]{1,0:T(8,128)} %refs_1_.1, f32[704,512]{1,0:T(8,128)} %refs_2_.1, f32[1,1408,512]{2,1,0:T(8,128)} %refs_3_.1, ...), custom_call_target="tpu_custom_call" | custom-call | tf_op jit(solution)/shard_map/orthogonal/pallas_call | solution.py:680
  235.3 0.0 copy-start.2
  235.3 2.7 %copy.21 = f32[704,512]{1,0:T(8,128)} copy(f32[704,512]{1,0:T(8,128)} %get-tuple-element.12) | data formatting | bytes 2883584
  238.0 0.0 copy-done.2
  238.0 0.0 copy-start.1
  238.0 1.1 copy.22
  239.1 0.8 copy-done.1
  239.9 0.0 copy-start
  239.9 1.1 copy.23
  241.0 0.8 copy-done
  241.8 0.0 copy-start.4
  241.8 0.0 copy-start.3
  241.8 1.1 copy.24
  242.9 0.0 copy-done.4
  242.9 0.7 copy.25
  243.6 0.0 copy-done.3
  243.6 0.7 copy.26
Async XLA Ops:
  235.3 2.7 %copy-start.2 = (f32[704,512]{1,0:T(8,128)S(1)}, f32[704,512]{1,0:T(8,128)}, u32[]{:S(2)}) copy-start(f32[704,512]{1,0:T(8,128)} %get-tuple-element.13) | copy-start | bytes 4325380
  238.0 1.9 copy-start.1
  239.9 1.9 copy-start
  241.8 1.1 copy-start.4
  241.8 1.8 copy-start.3

commit v2 on v1

--- a/solution.py
+++ b/solution.py
@@ -47,6 +47,7 @@
     (c0, c1, c2, qs, qt, qtb, sums) = refs[33:40]
     (loc, rep_s, rep_r, ring_s, ring_r, half_s, half_r, in_s, in_r, mid_r) = refs[40:50]
     (out_s, out_r, ag_s, ag_r, dd_s, dd_r, gd_s, gd_r, pr_s, pr_r, q_s, q_r) = refs[50:62]
+    (x_s, x_r, st_s, st_r, sd_s, sd_r) = refs[62:68]
 
     height, size = s.shape[1:]
     width = size // ntp
@@ -336,6 +337,8 @@
 
     for m in range(3):
         left(txs[m], rep_s.at[m])
+    for d in range(1, ntp):
+        ring_b(d)
     for e in (3, 5, 8, 4, 6, 9, 7):
         here = spot(owners[e], kinds[e], side, r)
         arrived(here, ag_r.at[e])
@@ -383,8 +386,6 @@
     ring(0, ntp - 1)
     ring(1, 1)
     ring(side, 2)
-    for d in range(1, ntp):
-        ring_b(d)
     for m in range(3):
         local(speed[m], outs_m[m], 9 + m).wait()
         local(weights[m], speed[m], 12 + m).start()
@@ -453,8 +454,6 @@
 
     def poly_two(acc, lhs, rows, cols, shift):
         return eye(acc.shape, shift) + COEF_THREE * lhs[rows, cols].astype(F32) + COEF_FIVE * acc
-
-    product(0, b0, b0, b1, poly_one(inverse))
 
     for d in range(1, ntp):
         arrived(sb.at[:, at(peers[ntp - d] * thin, thin, thin)], ring_r.at[2, d])
@@ -470,15 +469,19 @@
             ).astype(BF16)
 
         exchange(b, 5 + b, make)
-    product(1, b0, b1, b2, times(inverse))
+    product(0, b0, b0, b1, poly_one(inverse))
+
     for b in range(blocks):
         chain_a(b, 5 + b)
+    product(1, b0, b1, b2, times(inverse))
+    chain_b(0, 5)
     product(2, b2, b1, b0, plain)
-    for b in range(blocks):
-        chain_b(b, 5 + b)
+    chain_b(1, 6)
+    chain_c(0, 5)
     product(3, b0, b0, b2, poly_two)
-    for b in range(blocks):
-        chain_c(b, 5 + b)
+    chain_b(2, 7)
+    chain_b(3, 8)
+    chain_c(1, 6)
 
     def panel(lhs, rhs, out, span, finish):
         def step(j, carry):
@@ -492,54 +495,73 @@
     def same(acc, cols):
         return acc
 
-    def factor(begin, g2, p1, p2, span, scaling, out):
+    def factor(rows, begin, extra, g2, p1, p2, span, scaling, out, tasks):
         def buf(ref):
-            return lambda: ref[:, :span]
+            return lambda: ref[:rows, :span]
 
         def put(ref):
             def write(cols, value):
-                ref[:, cols] = value
+                ref[:rows, cols] = value
 
             return write
 
         def cubic(acc, cols):
-            shift = cols.start - begin
-            return (
-                eye(acc.shape, shift)
-                + COEF_THREE * c1[:, cols].astype(F32)
-                + COEF_FIVE * acc
-            )
-
-        panel(lambda: p2(at(begin, half, half), None), lambda c: p2(None, c), put(c0), span, same)
-        panel(buf(c0), lambda c: g2(None, c), put(c1), span, same)
-        panel(buf(c1), lambda c: g2(None, c), put(c2), span, same)
-        panel(buf(c2), lambda c: p2(None, c), put(c0), span, same)
-        panel(buf(c0), lambda c: p2(None, c), put(c2), span, cubic)
-        panel(buf(c2), lambda c: p2(None, c), put(c0), span, same)
-        panel(buf(c0), lambda c: p1(None, c), out, span, lambda acc, cols: acc * scaling)
+            down = lax.broadcasted_iota(jnp.int32, acc.shape, 0)
+            over = lax.broadcasted_iota(jnp.int32, acc.shape, 1)
+            down = down + jnp.where(down < half, begin, extra - half)
+            unit = jnp.where(down == over + cols.start, COEF_ONE, 0.0)
+            return unit + COEF_THREE * c1[:rows, cols].astype(F32) + COEF_FIVE * acc
+
+        panel(buf(c2), p2, put(c0), span, same)
+        tasks(0)
+        panel(buf(c0), g2, put(c1), span, same)
+        tasks(1)
+        panel(buf(c1), g2, put(c2), span, same)
+        tasks(2)
+        panel(buf(c2), p2, put(c0), span, same)
+        tasks(3)
+        panel(buf(c0), p2, put(c2), span, cubic)
+        tasks(4)
+        panel(buf(c2), p2, put(c0), span, same)
+        tasks(5)
+        panel(buf(c0), p1, out, span, lambda acc, cols: acc * scaling)
 
     def view(ref, top, span):
-        def read(rows, cols):
-            if rows is None:
-                return ref[top : top + span, cols]
-            return ref[at(top + rows.start, half, half), :span]
-
-        return read
-
-    big = (view(b0, 0, size), view(b1, 0, size), view(b2, 0, size))
-
-    def put_qs(cols, value):
-        qs[:, cols] = value
-
-    def put_qt(cols, value):
-        qt[side, at(r * half, half, half), cols] = value
+        return lambda cols: ref[top : top + span, cols]
+
+    slab = half // nfs
+    begin, extra = t * width + r * half, across * width + r * half + f * slab
+
+    def put_q(cols, value):
+        qt[side, at(r * half, half, half), cols] = value[:half]
+        qs[:, cols] = value[half:]
 
     def put_qb(cols, value):
         qtb[:, cols] = value
 
-    factor(across * width + r * half, *big, size, scale, put_qs)
+    def fill(rows):
+        c2[rows, :] = b2[at(begin + rows.start, STEP, STEP), :]
+
+    rows_loop(half, STEP, fill)
+    c2[half : half + slab, :] = b2[at(extra, slab, slab), :]
+
+    def tasks(n):
+        if n == 1:
+            chain_c(2, 7)
+        if n == 3:
+            chain_c(3, 8)
+
+    factor(
+        half + slab, begin, extra, view(b0, 0, size), view(b1, 0, size), view(b2, 0, size),
+        size, scale, put_q, tasks,
+    )
+
+    def strip(m, who, j):
+        return qt.at[m, at(who * half + j * slab, slab, slab)]
+
+    send(qs, strip(side, r, f), x_s, x_r, {"tp": across}).start()
     landing = qt.at[side, at(r * half, half, half)]
-    send(qs, landing, q_s.at[0], q_r.at[0], {"tp": across}).start()
+    send(landing, landing, q_s, q_r, mate).start()
     for b in range(blocks):
         chain_d(b, 5 + b)
         a, c = b // wide_b, b % wide_b
@@ -551,8 +573,62 @@
 
         rows_loop(half, STEP, copy)
         send(tot.at[b], here, gd_s.at[b], gd_r.at[b], mate).start()
-    factor(t * width + r * half, *big, size, scale, put_qt)
-    send(landing, landing, q_s.at[1], q_r.at[1], mate).start()
+
+    def pass_on(d, up):
+        here = strip(1 - side, r, f)
+        from_far = d > 0
+        j = f - d if up else f + d
+        ahead = f + 1 if up else f - 1
+        inside = jnp.logical_and(j >= 0, j < nfs)
+        more = jnp.logical_and(ahead >= 0, ahead < nfs)
+        lane = 0 if up else 1
+        if from_far:
+            @pl.when(inside)
+            def _():
+                spot = strip(1 - side, r, j)
+                arrived(spot, st_r.at[lane, d])
+                send(spot, spot, sd_s.at[lane, d], sd_r.at[lane, d], mate).start()
+
+                @pl.when(more)
+                def _():
+                    send(
+                        spot, spot, st_s.at[lane, d], st_r.at[lane, d + 1], {"fs": ahead}
+                    ).start()
+        else:
+            @pl.when(more)
+            def _():
+                send(here, here, st_s.at[lane, 0], st_r.at[lane, 1], {"fs": ahead}).start()
+
+    def travel(d):
+        if d == 0:
+            here = strip(1 - side, r, f)
+            arrived(here, x_r)
+            pass_on(0, True)
+            pass_on(0, False)
+            send(here, here, sd_s.at[0, 0], sd_r.at[0, 0], mate).start()
+            return
+        pass_on(d, True)
+        pass_on(d, False)
+
+    def travelled(up, d):
+        j = f - d if up else f + d
+        lane = 0 if up else 1
+
+        @pl.when(jnp.logical_and(j >= 0, j < nfs))
+        def _():
+            spot = strip(1 - side, other, j)
+            arrived(spot, sd_r.at[lane, d])
+            left(spot, sd_s.at[lane, d])
+
+    def sent_on(up, d):
+        j = f - d if up else f + d
+        ahead = f + 1 if up else f - 1
+        lane = 0 if up else 1
+        inside = jnp.logical_and(j >= 0, j < nfs)
+        more = jnp.logical_and(ahead >= 0, ahead < nfs)
+        pl.when(jnp.logical_and(inside, more))(
+            lambda: left(strip(1 - side, r, j), st_s.at[lane, d])
+        )
 
     for b in range(blocks):
         a, c = b // wide_b, b % wide_b
@@ -579,10 +655,20 @@
 
     square(gb, gb, b1, poly_one(inverse_b))
     square(gb, b1, b2, times(inverse_b))
+    travel(0)
     square(b2, b1, b0, plain)
     square(b0, b0, b2, poly_two)
-    tiny = (view(b0, 0, small), view(b1, 0, small), view(b2, 0, small))
-    factor(t * thin, *tiny, small, scale_b, put_qb)
+    travel(1)
+    c2[:thin, :small] = b2[at(t * thin, thin, thin), :small]
+
+    def tasks_b(n):
+        if n == 3 and nfs > 2:
+            travel(2)
+
+    factor(
+        thin, t * thin, 0, view(b0, 0, small), view(b1, 0, small), view(b2, 0, small),
+        small, scale_b, put_qb, tasks_b,
+    )
 
     def update(m, lhs, rhs, rate, ref, rows_of, step):
         def body(rows):
@@ -623,12 +709,14 @@
     ring_in(0, ntp - 1)
     ring_in(1, 1)
     ring_in(1 - side, 2)
-    arrived(qt.at[side, at(other * half, half, half)], q_r.at[1])
+    arrived(qt.at[side, at(other * half, half, half)], q_r)
     finish_big(side)
-    far = qt.at[1 - side, at(r * half, half, half)]
-    arrived(far, q_r.at[0])
-    send(far, far, q_s.at[2], q_r.at[2], mate).start()
-    arrived(qt.at[1 - side, at(other * half, half, half)], q_r.at[2])
+    for d in range(3, nfs):
+        travel(d)
+    travelled(True, 0)
+    for d in range(1, nfs):
+        travelled(True, d)
+        travelled(False, d)
     finish_big(1 - side)
 
     for m in range(3):
@@ -638,12 +726,39 @@
     for b in range(blocks):
         chain_end(b, 5 + b)
         left(tot.at[b], gd_s.at[b])
-    left(qs, q_s.at[0])
-    left(landing, q_s.at[1])
-    left(far, q_s.at[2])
+    left(qs, x_s)
+    left(landing, q_s)
+    for d in range(nfs - 1):
+        sent_on(True, d)
+        sent_on(False, d)
     local(speed[0], gu, 15).wait()
     local(speed[1], uu, 16).wait()
     local(velb, bu, 17).wait()
+
+
+def hand_over(*refs):
+    count = (len(refs) - 2) // 3
+    sources, targets, stages = refs[:count], refs[count : 2 * count], refs[2 * count : 3 * count]
+    came, went = refs[3 * count :]
+    moves = []
+    for i in range(count):
+        rows = sources[i].shape[0]
+        for j, top in enumerate((0, rows // 2)):
+            span = pl.ds(top, rows // 2)
+            stage = stages[i].at[span]
+            moves.append(
+                (
+                    pltpu.make_async_copy(sources[i].at[span], stage, came.at[i, j]),
+                    pltpu.make_async_copy(stage, targets[i].at[span], went.at[i, j]),
+                )
+            )
+    for take, _ in moves:
+        take.start()
+    for take, give in moves:
+        take.wait()
+        give.start()
+    for _, give in moves:
+        give.wait()
 
 
 def local_part(nfs, ntp, *args):
@@ -667,17 +782,17 @@
     scratch += [vmem((5, half, width), BF16)] * 4
     scratch += [vmem((5 + blocks, half, width), BF16), vmem((5, half, width), BF16)]
     scratch += [vmem((size, size), BF16)] * 3 + [vmem((small, small), BF16)]
-    scratch += [vmem((half, size), BF16)] * 4
+    scratch += [vmem((half + half // nfs, size), BF16)] * 3 + [vmem((half // nfs, size), BF16)]
     scratch += [vmem((2, width, size), BF16), vmem((thin, small), BF16), vmem((2, 8, width), F32)]
     slots = dma((5 + blocks,))
     scratch += [dma((18,)), dma((3,)), dma((3,)), dma((3, ntp)), dma((3, ntp))]
     scratch += [slots] * 7
     scratch += [dma((5, 2)), dma((10,)), dma((10,)), dma((10,)), dma((blocks,)), dma((blocks,))]
-    scratch += [dma((4, 5)), dma((4, 5)), dma((3,)), dma((3,))]
+    scratch += [dma((4, 5)), dma((4, 5))] + [dma] * 4 + [dma((2, nfs))] * 4
     outs = []
     for i in range(3):
         outs += [jax.ShapeDtypeStruct(args[3 * i + 1].shape, F32)] * 2
-    return pl.pallas_call(
+    results = pl.pallas_call(
         functools.partial(kernel, nfs, ntp),
         out_shape=tuple(outs),
         in_specs=[pl.BlockSpec(memory_space=pl.ANY)] * 9,
@@ -688,6 +803,15 @@
         ),
         name="orthogonal",
     )(*args)
+    dma2 = dma((len(outs), 2))
+    return pl.pallas_call(
+        hand_over,
+        out_shape=tuple(outs),
+        in_specs=[pl.BlockSpec(memory_space=pl.ANY)] * len(outs),
+        out_specs=tuple([pl.BlockSpec(memory_space=pl.ANY)] * len(outs)),
+        scratch_shapes=[vmem(o.shape, F32) for o in outs] + [dma2, dma2],
+        name="hand_over",
+    )(*results)
 
 
 def solution(mesh):

time: 246 us -> 188 us (0.76)
  Pallas kernels: 235 us -> 187 us
  local copies, waits for them, and re-layouts: 8.96 us -> 0 us
    pallas_call x1, Pallas kernels: 235 us -> 181 us  [local_part(): pl.pallas_call(functools.partial(kernel, nfs, ntp), out_shape=tuple(outs)...]
    unnamed x16 -> x0, local copies, waits for them, and re-layouts: 8.96 us -> none
    pallas_call x0 -> x1, Pallas kernels: none -> 5.32 us  [local_part(): pl.pallas_call(hand_over, out_shape=tuple(outs), in_specs=[pl.BlockSpec(m...]
where the time goes in v2:
time: 188 us; the launch traced here: 187 us
  Pallas kernels  187 us (99%)
    pallas_call x1, Pallas kernels, local_part(): pl.pallas_call(functools.partial(kernel, nfs, ntp), out_shape=tuple(outs)...  181 us
    pallas_call x1, Pallas kernels, local_part(): pl.pallas_call(hand_over, out_shape=tuple(outs), in_specs=[pl.BlockSpec(m...  5.32 us

profile of v2, /device:TPU:7, one launch (start us, length us, event | category | flops | bytes accessed | tf_op | source)
XLA Modules:
  0.0 187.3 jit_solution(10280591690831835325)
XLA Ops:
  0.6 181.2 %orthogonal.1 = (f32[704,512]{1,0:T(8,128)}, f32[704,512]{1,0:T(8,128)}, f32[704,512]{1,0:T(8,128)}, f32[704,512]{1,0:T(8,128)}, f32[256,256]{1,0:T(8,128)}, /*index=5*/f32[256,256]{1,0:T(8,128)}) custom-call(f32[1,1408,512]{2,1,0:T(8,128)} %refs_0_.1, f32[704,512]{1,0:T(8,128)} %refs_1_.1, f32[704,512]{1,0:T(8,128)} %refs_2_.1, f32[1,1408,512]{2,1,0:T(8,128)} %refs_3_.1, ...), custom_call_target="tpu_custom_call" | custom-call | tf_op jit(solution)/shard_map/orthogonal/pallas_call | solution.py:795
  181.8 5.3 %hand_over.1 = (f32[704,512]{1,0:T(8,128)}, f32[704,512]{1,0:T(8,128)}, f32[704,512]{1,0:T(8,128)}, f32[704,512]{1,0:T(8,128)}, f32[256,256]{1,0:T(8,128)}, /*index=5*/f32[256,256]{1,0:T(8,128)}) custom-call(f32[704,512]{1,0:T(8,128)} %get-tuple-element.12.refs_0_, f32[704,512]{1,0:T(8,128)} %get-tuple-element.13.refs_1_, ...), custom_call_target="tpu_custom_call" | custom-call | tf_op jit(solution)/shard_map/hand_over/pallas_call | solution.py:807

commit v3 on v2

--- a/solution.py
+++ b/solution.py
@@ -194,57 +194,75 @@
 
         exchange(slot, slot, make)
 
-    def add_into(b, ref):
+    shares = {0: 1, 1: 2, 2: 4}
+
+    def cut(c, n):
+        return pl.ds(c * (half // n), half // n)
+
+    def add_into(out, b, span, ref):
         def add(rows):
+            rows = at(span.start + rows.start, rows.size, rows.size)
             value = part[b, rows, :].astype(F32) + ref[rows, :].astype(F32)
-            part[b, rows, :] = value.astype(BF16)
-
-        rows_loop(half, STEP, add)
-
-    def to_inner(b, i):
-        send(part.at[b], rin.at[b], in_s.at[i], in_r.at[i], {"fs": inward}).start()
-
-    def to_outer(b, i):
-        send(tot.at[b], tot.at[b], out_s.at[i], out_r.at[i], {"fs": outward}).start()
-
-    def chain_a(b, i):
+            out[b, rows, :] = value.astype(BF16)
+
+        rows_loop(span.size, STEP, add)
+
+    def to_inner(b, i, c, n):
+        src, dst = part.at[b, cut(c, n)], rin.at[b, cut(c, n)]
+        send(src, dst, in_s.at[i, c], in_r.at[i, c], {"fs": inward}).start()
+
+    def to_outer(b, i, c, n):
+        src = tot.at[b, cut(c, n)]
+        send(src, src, out_s.at[i, c], out_r.at[i, c], {"fs": outward}).start()
+
+    def chain_a(b, i, n=1):
         arrived(prcv.at[b], half_r.at[i])
-        add_into(b, prcv.at[b])
-        pl.when(jnp.logical_and(is_end, jnp.logical_not(is_mid)))(lambda: to_inner(b, i))
-
-    def chain_b(b, i):
+        for c in range(n):
+            add_into(part, b, cut(c, n), prcv.at[b])
+            pl.when(jnp.logical_and(is_end, jnp.logical_not(is_mid)))(
+                lambda c=c: to_inner(b, i, c, n)
+            )
+
+    def chain_b(b, i, c=0, n=1):
+        span = cut(c, n)
+
         @pl.when(jnp.logical_not(is_end))
         def _():
-            arrived(rin.at[b], in_r.at[i])
-            add_into(b, rin.at[b])
-            pl.when(jnp.logical_not(is_mid))(lambda: to_inner(b, i))
+            arrived(rin.at[b, span], in_r.at[i, c])
+            add_into(part, b, span, rin.at[b])
+            pl.when(jnp.logical_not(is_mid))(lambda: to_inner(b, i, c, n))
 
         @pl.when(is_mid)
         def _():
-            send(part.at[b], cross.at[i], in_s.at[i], mid_r.at[i], {"fs": inward}).start()
-
-    def chain_c(b, i):
+            src, dst = part.at[b, span], cross.at[i, span]
+            send(src, dst, in_s.at[i, c], mid_r.at[i, c], {"fs": inward}).start()
+
+    def chain_c(b, i, c=0, n=1, then=None):
+        span = cut(c, n)
+
         @pl.when(is_mid)
         def _():
-            arrived(cross.at[i], mid_r.at[i])
-
-            def add(rows):
-                value = part[b, rows, :].astype(F32) + cross[i, rows, :].astype(F32)
-                tot[b, rows, :] = value.astype(BF16)
-
-            rows_loop(half, STEP, add)
-            pl.when(jnp.logical_not(is_end))(lambda: to_outer(b, i))
-
-    def chain_d(b, i):
+            arrived(cross.at[i, span], mid_r.at[i, c])
+            add_into(tot, b, span, cross.at[i])
+            pl.when(jnp.logical_not(is_end))(lambda: to_outer(b, i, c, n))
+            if then is not None:
+                then(b, c)
+
+    def chain_d(b, i, c=0, n=1, then=None):
         @pl.when(jnp.logical_not(is_mid))
         def _():
-            arrived(tot.at[b], out_r.at[i])
-            pl.when(jnp.logical_not(is_end))(lambda: to_outer(b, i))
-
-    def chain_end(b, i):
+            arrived(tot.at[b, cut(c, n)], out_r.at[i, c])
+            pl.when(jnp.logical_not(is_end))(lambda: to_outer(b, i, c, n))
+            if then is not None:
+                then(b, c)
+
+    def chain_end(b, i, n=1):
         left(psend.at[b], half_s.at[i])
-        left(part.at[b], in_s.at[i])
-        pl.when(jnp.logical_not(is_end))(lambda: left(tot.at[b], out_s.at[i]))
+        for c in range(n):
+            left(part.at[b, cut(c, n)], in_s.at[i, c])
+            pl.when(jnp.logical_not(is_end))(
+                lambda c=c: left(tot.at[b, cut(c, n)], out_s.at[i, c])
+            )
 
     def place(q, kind, matrix):
         a = turn(q)
@@ -255,45 +273,49 @@
         }[kind]
         return jnp.minimum(a, b), jnp.maximum(a, b)
 
-    def spot(q, kind, matrix, h):
+    def spot(q, kind, matrix, h, c=0, n=1):
         i, j = place(q, kind, matrix)
-        return b0.at[at(i * width + h * half, half, half), at(j * width, width, width)]
+        top = i * width + h * half + c * (half // n)
+        return b0.at[at(top, half // n, half // n), at(j * width, width, width)]
 
     kinds = (0, 1, 2, 0, 1, 0, 1, 2, 0, 1)
     owners = [p] * 3 + [turn(across)] * 2 + [turn(beside)] * 3 + [turn(diagonal)] * 2
 
-    def gather_own(slot, kind, matrix):
-        here = spot(p, kind, matrix, r)
+    def gather_own(slot, kind, matrix, c):
+        n = shares[kind]
+        here, src = spot(p, kind, matrix, r, c, n), tot.at[slot, cut(c, n)]
         i, j = place(p, kind, matrix)
+        top = c * (half // n)
 
         def copy(rows):
-            start = i * width + r * half
-            b0[at(start + rows.start, STEP, STEP), at(j * width, width, width)] = tot[
-                slot, rows, :
+            to = at(i * width + r * half + top + rows.start, rows.size, rows.size)
+            b0[to, at(j * width, width, width)] = tot[
+                slot, at(top + rows.start, rows.size, rows.size), :
             ]
 
-        rows_loop(half, STEP, copy)
+        rows_loop(half // n, STEP, copy)
         send(
-            tot.at[slot], here, ag_s.at[slot, 0], ag_r.at[5 + kind], {"tp": beside}
+            src, here, ag_s.at[slot, c, 0], ag_r.at[5 + kind, c], {"tp": beside}
         ).start()
-        send(tot.at[slot], here, dd_s.at[kind], dd_r.at[kind], mate).start()
-
-    def gather_far(slot, kind, matrix):
-        here = spot(p, kind, matrix, r)
+        send(src, here, dd_s.at[kind, c], dd_r.at[kind, c], mate).start()
+
+    def gather_far(slot, kind, matrix, c):
+        n = shares[kind]
+        here, src = spot(p, kind, matrix, r, c, n), tot.at[slot, cut(c, n)]
         send(
-            tot.at[slot], here, ag_s.at[slot, 0], ag_r.at[3 + kind], {"tp": across}
+            src, here, ag_s.at[slot, c, 0], ag_r.at[3 + kind, c], {"tp": across}
         ).start()
         send(
-            tot.at[slot], here, ag_s.at[slot, 1], ag_r.at[8 + kind], {"tp": diagonal}
+            src, here, ag_s.at[slot, c, 1], ag_r.at[8 + kind, c], {"tp": diagonal}
         ).start()
 
-    def gather(slot):
+    def gather(slot, c):
         if slot == 4:
-            gather_own(slot, 2, side)
+            gather_own(slot, 2, side, c)
             return
         matrix, kind = slot // 2, slot % 2
-        pl.when(side == matrix)(lambda: gather_own(slot, kind, matrix))
-        pl.when(side != matrix)(lambda: gather_far(slot, kind, matrix))
+        pl.when(side == matrix)(lambda: gather_own(slot, kind, matrix, c))
+        pl.when(side != matrix)(lambda: gather_far(slot, kind, matrix, c))
 
     momentum(0)
     ring(0, 1)
@@ -311,38 +333,42 @@
     gram(1, 0, peers[ntp - 1], t)
     ring_in(1, ntp - 1)
     gram(3, 1, peers[1], t)
-    chain_a(1, 1)
-    chain_a(3, 3)
-    chain_c(0, 0)
-    chain_c(2, 2)
-    chain_b(1, 1)
-    chain_b(3, 3)
-    chain_d(0, 0)
-    gather(0)
-    chain_d(2, 2)
-    gather(2)
+    few, many = shares[1], shares[2]
+    chain_a(1, 1, few)
+    chain_a(3, 3, few)
+    chain_c(0, 0, then=gather)
+    chain_c(2, 2, then=gather)
+    for slot in (1, 3):
+        for c in range(few):
+            chain_b(slot, slot, c, few)
+    chain_d(0, 0, then=gather)
+    chain_d(2, 2, then=gather)
     ring_in(side, 2)
     gram(4, side, peers[2], t)
-    chain_a(4, 4)
-    chain_c(1, 1)
-    chain_c(3, 3)
-    chain_b(4, 4)
-    chain_d(1, 1)
-    gather(1)
-    chain_d(3, 3)
-    gather(3)
-    chain_c(4, 4)
-    chain_d(4, 4)
-    gather(4)
+    chain_a(4, 4, many)
+    for slot in (1, 3):
+        for c in range(few):
+            chain_c(slot, slot, c, few, gather)
+    for c in range(many + 1):
+        if c < many:
+            chain_b(4, 4, c, many)
+        if c > 0:
+            chain_c(4, 4, c - 1, many, gather)
+    for slot in (1, 3):
+        for c in range(few):
+            chain_d(slot, slot, c, few, gather)
+    for c in range(many):
+        chain_d(4, 4, c, many, gather)
 
     for m in range(3):
         left(txs[m], rep_s.at[m])
-    for d in range(1, ntp):
-        ring_b(d)
-    for e in (3, 5, 8, 4, 6, 9, 7):
-        here = spot(owners[e], kinds[e], side, r)
-        arrived(here, ag_r.at[e])
-        send(here, here, dd_s.at[e], dd_r.at[e], mate).start()
+
+    def forward(e):
+        n = shares[kinds[e]]
+        for c in range(n):
+            here = spot(owners[e], kinds[e], side, r, c, n)
+            arrived(here, ag_r.at[e, c])
+            send(here, here, dd_s.at[e, c], dd_r.at[e, c], mate).start()
 
     sums[...] = jnp.zeros_like(sums)
 
@@ -367,8 +393,10 @@
         ratio = SAFETY * (second + 1.0) / (first + 1.0)
         return 1.0 / ratio, lax.rsqrt(ratio)
 
-    for e in range(10):
-        arrived(spot(owners[e], kinds[e], side, other), dd_r.at[e])
+    def digest(e):
+        n = shares[kinds[e]]
+        for c in range(n):
+            arrived(spot(owners[e], kinds[e], side, other, c, n), dd_r.at[e, c])
         i, j = place(owners[e], kinds[e], side)
         survey(b0, i * width, j * width, kinds[e] == 0, width)
         if kinds[e] != 0:
@@ -376,13 +404,34 @@
                 at(i * width, width, width), at(j * width, width, width)
             ].T
 
+    for e in (3, 5, 8):
+        forward(e)
+    for e in (0, 3, 5, 8):
+        digest(e)
+    for e in (4, 6, 9):
+        forward(e)
+    for e in (1, 4, 6, 9):
+        digest(e)
+    forward(7)
+    digest(2)
+    digest(7)
+
     for slot in range(5):
-        left(tot.at[slot], ag_s.at[slot, 0])
-        if slot < 4:
-            pl.when(side != slot // 2)(lambda slot=slot: left(tot.at[slot], ag_s.at[slot, 1]))
-        chain_end(slot, slot)
+        n = shares[2] if slot == 4 else shares[slot % 2]
+        chain_end(slot, slot, n)
+        for c in range(n):
+            piece = tot.at[slot, cut(c, n)]
+            left(piece, ag_s.at[slot, c, 0])
+            if slot < 4:
+                pl.when(side != slot // 2)(
+                    lambda piece=piece, slot=slot, c=c: left(piece, ag_s.at[slot, c, 1])
+                )
     for e in range(10):
-        left(tot.at[0], dd_s.at[e])
+        n = shares[kinds[e]]
+        for c in range(n):
+            left(tot.at[0, cut(0, n)], dd_s.at[e, c])
+    for d in range(1, ntp):
+        ring_b(d)
     ring(0, ntp - 1)
     ring(1, 1)
     ring(side, 2)
@@ -397,36 +446,32 @@
         over = lax.broadcasted_iota(jnp.int32, shape, 1)
         return jnp.where(down == over + shift, COEF_ONE, 0.0)
 
-    def product(index, lhs, rhs, out, finish):
+    def product(index, span, lhs, rhs, out, finish, before, after=None):
+        step = span // count
+
         def where(k, who):
-            third, fourth = k // 3, k // 4
-            i, j = third - fourth, k - 2 * third + fourth
-            i, j = (
-                i + who * (3 - j + fourth - i),
-                j + who * (3 - i - fourth - j),
-            )
-            return i, j
-
-        def step(k, carry):
-            i, j = where(k, r)
-            rows, cols = at(i * tile, tile, tile), at(j * tile, tile, tile)
-            acc = jnp.dot(lhs[rows, :], rhs[:, cols], preferred_element_type=F32)
-            value = finish(acc, lhs, rows, cols, (j - i) * tile).astype(BF16)
+            i, j = k // 4, jnp.where(k == 1, 3, jnp.where(k > 1, k - 1 - k // 4 * 2, 0))
+            odd = jnp.where(k == 1, 1, 0)
+            i, j = i + who * (3 - j + odd - i), j + who * (3 - i - odd - j)
+            return i, j, at(i * step, step, step), at(j * step, step, step)
+
+        def compute(k):
+            i, j, rows, cols = where(k, r)
+            acc = jnp.dot(lhs[rows, :span], rhs[:span, cols], preferred_element_type=F32)
+            value = finish(acc, lhs, rows, cols, (j - i) * step).astype(BF16)
             out[rows, cols] = value
-            here = out.at[rows, cols]
-            send(here, here, pr_s.at[index, k], pr_r.at[index, k], mate).start()
 
             @pl.when(i != j)
             def _():
                 out[cols, rows] = value.T
 
-            return carry
-
-        lax.fori_loop(0, 5, step, 0)
-
-        def take(k, carry):
-            i, j = where(k, other)
-            rows, cols = at(i * tile, tile, tile), at(j * tile, tile, tile)
+        def ship(k):
+            _, _, rows, cols = where(k, r)
+            here = out.at[rows, cols]
+            send(here, here, pr_s.at[index, k], pr_r.at[index, k], mate).start()
+
+        def take(k):
+            i, j, rows, cols = where(k, other)
             here = out.at[rows, cols]
             arrived(here, pr_r.at[index, k])
 
@@ -435,9 +480,26 @@
                 out[cols, rows] = out[rows, cols].T
 
             left(here, pr_s.at[index, k])
+
+        compute(0)
+        before()
+        ship(0)
+
+        def run(k, carry):
+            compute(k)
+            ship(k)
             return carry
 
-        lax.fori_loop(0, 5, take, 0)
+        lax.fori_loop(1, 5, run, 0)
+        if after is not None:
+            after()
+        take(1)
+
+        def rest(n, carry):
+            take(n + jnp.minimum(n, 1))
+            return carry
+
+        return lambda: lax.fori_loop(0, 4, rest, 0)
 
     def poly_one(inv):
         def finish(acc, lhs, rows, cols, shift):
@@ -455,33 +517,53 @@
     def poly_two(acc, lhs, rows, cols, shift):
         return eye(acc.shape, shift) + COEF_THREE * lhs[rows, cols].astype(F32) + COEF_FIVE * acc
 
-    for d in range(1, ntp):
-        arrived(sb.at[:, at(peers[ntp - d] * thin, thin, thin)], ring_r.at[2, d])
-    deep, wide_b = small // 2 // half, small // width
-    blocks = deep * wide_b
-    for b in range(blocks):
-        def make(h, b=b):
-            return lax.dot_general(
-                sb[:, at(h * (small // 2) + b // wide_b * half, half, half)],
-                sb[:, b % wide_b * width : (b % wide_b + 1) * width],
-                (((0,), (0,)), ((), ())),
-                preferred_element_type=F32,
-            ).astype(BF16)
-
-        exchange(b, 5 + b, make)
-    product(0, b0, b0, b1, poly_one(inverse))
-
-    for b in range(blocks):
-        chain_a(b, 5 + b)
-    product(1, b0, b1, b2, times(inverse))
+    done = product(0, size, b0, b0, b1, poly_one(inverse), lambda: None)
+
+    blocks = 3
+
+    def block(b, who):
+        i, j = (2 * who + b, who) if b < 2 else (who, 1)
+        return i * half, j * width
+
+    def branch_gram():
+        for d in range(1, ntp):
+            arrived(sb.at[:, at(peers[ntp - d] * thin, thin, thin)], ring_r.at[2, d])
+        for b in range(blocks):
+            def make(who, b=b):
+                i, j = block(b, who)
+                return lax.dot_general(
+                    sb[:, at(i, half, half)],
+                    sb[:, at(j, width, width)],
+                    (((0,), (0,)), ((), ())),
+                    preferred_element_type=F32,
+                ).astype(BF16)
+
+            exchange(b, 5 + b, make)
+
+    def settle(b):
+        chain_d(b, 5 + b)
+        i, j = block(b, r)
+
+        def copy(rows):
+            gb[at(i + rows.start, STEP, STEP), at(j, width, width)] = tot[b, rows, :]
+
+        rows_loop(half, STEP, copy)
+        here = gb.at[at(i, half, half), at(j, width, width)]
+        send(tot.at[b], here, gd_s.at[b], gd_r.at[b], mate).start()
+
+    done = product(1, size, b0, b1, b2, times(inverse), done, branch_gram)
+
+    def begin_chain(first):
+        first()
+        for b in range(blocks):
+            chain_a(b, 5 + b)
+
+    done = product(2, size, b2, b1, b0, plain, functools.partial(begin_chain, done))
     chain_b(0, 5)
-    product(2, b2, b1, b0, plain)
+    done = product(3, size, b0, b0, b2, poly_two, done)
     chain_b(1, 6)
     chain_c(0, 5)
-    product(3, b0, b0, b2, poly_two)
-    chain_b(2, 7)
-    chain_b(3, 8)
-    chain_c(1, 6)
+    done()
 
     def panel(lhs, rhs, out, span, finish):
         def step(j, carry):
@@ -546,124 +628,112 @@
     c2[half : half + slab, :] = b2[at(extra, slab, slab), :]
 
     def tasks(n):
+        if n == 0:
+            chain_b(2, 7)
         if n == 1:
+            chain_c(1, 6)
+        if n == 2:
             chain_c(2, 7)
         if n == 3:
-            chain_c(3, 8)
+            settle(0)
+        if n == 5:
+            settle(1)
+            settle(2)
 
     factor(
         half + slab, begin, extra, view(b0, 0, size), view(b1, 0, size), view(b2, 0, size),
         size, scale, put_q, tasks,
     )
 
-    def strip(m, who, j):
-        return qt.at[m, at(who * half + j * slab, slab, slab)]
-
-    send(qs, strip(side, r, f), x_s, x_r, {"tp": across}).start()
+    chunk = size // 2
+
+    def strip(m, who, j, c):
+        return qt.at[m, at(who * half + j * slab, slab, slab), c * chunk : (c + 1) * chunk]
+
+    for c in range(2):
+        piece = qs.at[:, c * chunk : (c + 1) * chunk]
+        send(piece, strip(side, r, f, c), x_s.at[c], x_r.at[c], {"tp": across}).start()
     landing = qt.at[side, at(r * half, half, half)]
     send(landing, landing, q_s, q_r, mate).start()
-    for b in range(blocks):
-        chain_d(b, 5 + b)
-        a, c = b // wide_b, b % wide_b
-        start = r * (small // 2) + a * half
-        here = gb.at[at(start, half, half), c * width : (c + 1) * width]
-
-        def copy(rows, b=b, start=start, c=c):
-            gb[at(start + rows.start, STEP, STEP), c * width : (c + 1) * width] = tot[b, rows, :]
-
-        rows_loop(half, STEP, copy)
-        send(tot.at[b], here, gd_s.at[b], gd_r.at[b], mate).start()
-
-    def pass_on(d, up):
-        here = strip(1 - side, r, f)
-        from_far = d > 0
-        j = f - d if up else f + d
-        ahead = f + 1 if up else f - 1
+
+    def course(d, up):
+        j, ahead = (f - d, f + 1) if up else (f + d, f - 1)
         inside = jnp.logical_and(j >= 0, j < nfs)
         more = jnp.logical_and(ahead >= 0, ahead < nfs)
-        lane = 0 if up else 1
-        if from_far:
-            @pl.when(inside)
-            def _():
-                spot = strip(1 - side, r, j)
-                arrived(spot, st_r.at[lane, d])
-                send(spot, spot, sd_s.at[lane, d], sd_r.at[lane, d], mate).start()
-
-                @pl.when(more)
-                def _():
-                    send(
-                        spot, spot, st_s.at[lane, d], st_r.at[lane, d + 1], {"fs": ahead}
-                    ).start()
-        else:
-            @pl.when(more)
-            def _():
-                send(here, here, st_s.at[lane, 0], st_r.at[lane, 1], {"fs": ahead}).start()
-
-    def travel(d):
+        return 0 if up else 1, j, ahead, inside, more
+
+    def pass_on(d, c, up):
+        lane, j, ahead, inside, more = course(d, up)
+
+        def onward(spot):
+            send(
+                spot, spot, st_s.at[lane, 2 * d + c], st_r.at[lane, 2 * d + 2 + c], {"fs": ahead}
+            ).start()
+
         if d == 0:
-            here = strip(1 - side, r, f)
-            arrived(here, x_r)
-            pass_on(0, True)
-            pass_on(0, False)
-            send(here, here, sd_s.at[0, 0], sd_r.at[0, 0], mate).start()
+            pl.when(more)(lambda: onward(strip(1 - side, r, f, c)))
             return
-        pass_on(d, True)
-        pass_on(d, False)
-
-    def travelled(up, d):
-        j = f - d if up else f + d
-        lane = 0 if up else 1
-
-        @pl.when(jnp.logical_and(j >= 0, j < nfs))
+
+        @pl.when(inside)
         def _():
-            spot = strip(1 - side, other, j)
-            arrived(spot, sd_r.at[lane, d])
-            left(spot, sd_s.at[lane, d])
-
-    def sent_on(up, d):
-        j = f - d if up else f + d
-        ahead = f + 1 if up else f - 1
-        lane = 0 if up else 1
-        inside = jnp.logical_and(j >= 0, j < nfs)
-        more = jnp.logical_and(ahead >= 0, ahead < nfs)
+            spot = strip(1 - side, r, j, c)
+            arrived(spot, st_r.at[lane, 2 * d + c])
+            pl.when(more)(lambda: onward(spot))
+            send(
+                spot, spot, sd_s.at[lane, 2 * d + c], sd_r.at[lane, 2 * d + c], mate
+            ).start()
+
+    def travel(d, c):
+        if d >= nfs:
+            return
+        if d == 0:
+            arrived(strip(1 - side, r, f, c), x_r.at[c])
+        pass_on(d, c, True)
+        pass_on(d, c, False)
+        if d == 0:
+            here = strip(1 - side, r, f, c)
+            send(here, here, sd_s.at[0, c], sd_r.at[0, c], mate).start()
+
+    def travelled(d, c, up):
+        lane, j, ahead, inside, more = course(d, up)
+
+        @pl.when(inside)
+        def _():
+            spot = strip(1 - side, other, j, c)
+            arrived(spot, sd_r.at[lane, 2 * d + c])
+            left(spot, sd_s.at[lane, 2 * d + c])
+
+    def sent_on(d, c, up):
+        lane, j, ahead, inside, more = course(d, up)
         pl.when(jnp.logical_and(inside, more))(
-            lambda: left(strip(1 - side, r, j), st_s.at[lane, d])
+            lambda: left(strip(1 - side, r, j, c), st_s.at[lane, 2 * d + c])
         )
 
     for b in range(blocks):
-        a, c = b // wide_b, b % wide_b
-        start = other * (small // 2) + a * half
-        arrived(gb.at[at(start, half, half), c * width : (c + 1) * width], gd_r.at[b])
+        i, j = block(b, other)
+        arrived(gb.at[at(i, half, half), at(j, width, width)], gd_r.at[b])
     sums[...] = jnp.zeros_like(sums)
-    for i in range(0, small, width):
-        for j in range(0, small, width):
-            if i == j:
-                survey(gb, i, j, True, width)
-            if i < j:
-                survey(gb, i, j, False, width)
+    survey(gb, 0, 0, True, width)
+    survey(gb, width, width, True, width)
+    survey(gb, 0, width, False, width)
+    gb[width:, :width] = gb[:width, width:].T
     inverse_b, scale_b = scales()
-
-    def square(lhs, rhs, out, finish):
-        def step(n, carry):
-            i, j = n // (small // tile), n % (small // tile)
-            rows, cols = at(i * tile, tile, tile), at(j * tile, tile, tile)
-            acc = jnp.dot(lhs[rows, :small], rhs[:small, cols], preferred_element_type=F32)
-            out[rows, cols] = finish(acc, lhs, rows, cols, (j - i) * tile).astype(BF16)
-            return carry
-
-        lax.fori_loop(0, (small // tile) ** 2, step, 0)
-
-    square(gb, gb, b1, poly_one(inverse_b))
-    square(gb, b1, b2, times(inverse_b))
-    travel(0)
-    square(b2, b1, b0, plain)
-    square(b0, b0, b2, poly_two)
-    travel(1)
+    both = lambda: arrived(qt.at[side, at(other * half, half, half)], q_r)
+    done = product(4, small, gb, gb, b1, poly_one(inverse_b), both)
+    done = product(5, small, gb, b1, b2, times(inverse_b), done)
+    travel(0, 0)
+    done = product(6, small, b2, b1, b0, plain, done)
+    travel(0, 1)
+    done = product(7, small, b0, b0, b2, poly_two, done)
+    travel(1, 0)
+    done()
     c2[:thin, :small] = b2[at(t * thin, thin, thin), :small]
 
     def tasks_b(n):
-        if n == 3 and nfs > 2:
-            travel(2)
+        if n == 1:
+            travel(1, 1)
+        if n == 3:
+            travel(2, 0)
 
     factor(
         thin, t * thin, 0, view(b0, 0, small), view(b1, 0, small), view(b2, 0, small),
@@ -706,17 +776,19 @@
         local(weights[m], speed[m], 12 + m).wait()
     update(2, lambda rows: sb[rows, :], lambda: qtb[...], rate_b, put_small, low, CHUNK)
     local(velb, bu, 17).start()
+    travel(2, 1)
     ring_in(0, ntp - 1)
     ring_in(1, 1)
     ring_in(1 - side, 2)
-    arrived(qt.at[side, at(other * half, half, half)], q_r)
     finish_big(side)
     for d in range(3, nfs):
-        travel(d)
-    travelled(True, 0)
-    for d in range(1, nfs):
-        travelled(True, d)
-        travelled(False, d)
+        travel(d, 0)
+        travel(d, 1)
+    for d in range(nfs):
+        for c in range(2):
+            travelled(d, c, True)
+            if d > 0:
+                travelled(d, c, False)
     finish_big(1 - side)
 
     for m in range(3):
@@ -726,11 +798,12 @@
     for b in range(blocks):
         chain_end(b, 5 + b)
         left(tot.at[b], gd_s.at[b])
-    left(qs, x_s)
     left(landing, q_s)
-    for d in range(nfs - 1):
-        sent_on(True, d)
-        sent_on(False, d)
+    for c in range(2):
+        left(qs.at[:, c * chunk : (c + 1) * chunk], x_s.at[c])
+        for d in range(nfs - 1):
+            sent_on(d, c, True)
+            sent_on(d, c, False)
     local(speed[0], gu, 15).wait()
     local(speed[1], uu, 16).wait()
     local(velb, bu, 17).wait()
@@ -766,7 +839,7 @@
     low, thin = args[7].shape
     size, small = width * ntp, thin * ntp
     half = width // 2
-    blocks = small // 2 // half * (small // width)
+    blocks = 3
     vmem = pltpu.VMEM
     dma = pltpu.SemaphoreType.DMA
     scratch = [
@@ -786,9 +859,9 @@
     scratch += [vmem((2, width, size), BF16), vmem((thin, small), BF16), vmem((2, 8, width), F32)]
     slots = dma((5 + blocks,))
     scratch += [dma((18,)), dma((3,)), dma((3,)), dma((3, ntp)), dma((3, ntp))]
-    scratch += [slots] * 7
-    scratch += [dma((5, 2)), dma((10,)), dma((10,)), dma((10,)), dma((blocks,)), dma((blocks,))]
-    scratch += [dma((4, 5)), dma((4, 5))] + [dma] * 4 + [dma((2, nfs))] * 4
+    scratch += [slots] * 2 + [dma((5 + blocks, 4))] * 5
+    scratch += [dma((5, 4, 2)), dma((10, 4)), dma((10, 4)), dma((10, 4)), dma((blocks,)), dma((blocks,))]
+    scratch += [dma((8, 5))] * 2 + [dma, dma, dma((2,)), dma((2,))] + [dma((2, 2 * nfs))] * 4
     outs = []
     for i in range(3):
         outs += [jax.ShapeDtypeStruct(args[3 * i + 1].shape, F32)] * 2

time: 188 us -> 175 us (0.931)
  Pallas kernels: 187 us -> 174 us
    pallas_call x1, Pallas kernels: 181 us -> 169 us  [local_part(): pl.pallas_call(functools.partial(kernel, nfs, ntp), out_shape=tuple(outs)...]
where the time goes in v3:
time: 175 us
  Pallas kernels  174 us (99%)
    pallas_call x1, Pallas kernels, local_part(): pl.pallas_call(functools.partial(kernel, nfs, ntp), out_shape=tuple(outs)...  169 us
    pallas_call x1, Pallas kernels, local_part(): pl.pallas_call(hand_over, out_shape=tuple(outs), in_specs=[pl.BlockSpec(m...  5.32 us

profile of v3, /device:TPU:7, one launch (start us, length us, event | category | flops | bytes accessed | tf_op | source)
XLA Modules:
  0.0 175.2 jit_solution(6617987144904620409)
XLA Ops:
  0.6 169.1 %orthogonal.1 = (f32[704,512]{1,0:T(8,128)}, f32[704,512]{1,0:T(8,128)}, f32[704,512]{1,0:T(8,128)}, f32[704,512]{1,0:T(8,128)}, f32[256,256]{1,0:T(8,128)}, /*index=5*/f32[256,256]{1,0:T(8,128)}) custom-call(f32[1,1408,512]{2,1,0:T(8,128)} %refs_0_.1, f32[704,512]{1,0:T(8,128)} %refs_1_.1, f32[704,512]{1,0:T(8,128)} %refs_2_.1, f32[1,1408,512]{2,1,0:T(8,128)} %refs_3_.1, ...), custom_call_target="tpu_custom_call" | custom-call | tf_op jit(solution)/shard_map/orthogonal/pallas_call | solution.py:868
  169.8 5.3 %hand_over.1 = (f32[704,512]{1,0:T(8,128)}, f32[704,512]{1,0:T(8,128)}, f32[704,512]{1,0:T(8,128)}, f32[704,512]{1,0:T(8,128)}, f32[256,256]{1,0:T(8,128)}, /*index=5*/f32[256,256]{1,0:T(8,128)}) custom-call(f32[704,512]{1,0:T(8,128)} %get-tuple-element.12.refs_0_, f32[704,512]{1,0:T(8,128)} %get-tuple-element.13.refs_1_, ...), custom_call_target="tpu_custom_call" | custom-call | tf_op jit(solution)/shard_map/hand_over/pallas_call | solution.py:880

commit v4 on v3

--- a/solution.py
+++ b/solution.py
@@ -614,9 +614,19 @@
     slab = half // nfs
     begin, extra = t * width + r * half, across * width + r * half + f * slab
 
+    chunk = size // 2
+
+    def strip(m, who, j, c):
+        return qt.at[m, at(who * half + j * slab, slab, slab), c * chunk : (c + 1) * chunk]
+
+    def depart(c):
+        piece = qs.at[:, c * chunk : (c + 1) * chunk]
+        send(piece, strip(side, r, f, c), x_s.at[c], x_r.at[c], {"tp": across}).start()
+
     def put_q(cols, value):
         qt[side, at(r * half, half, half), cols] = value[:half]
         qs[:, cols] = value[half:]
+        pl.when(cols.start == chunk)(lambda: depart(0))
 
     def put_qb(cols, value):
         qtb[:, cols] = value
@@ -645,14 +655,7 @@
         size, scale, put_q, tasks,
     )
 
-    chunk = size // 2
-
-    def strip(m, who, j, c):
-        return qt.at[m, at(who * half + j * slab, slab, slab), c * chunk : (c + 1) * chunk]
-
-    for c in range(2):
-        piece = qs.at[:, c * chunk : (c + 1) * chunk]
-        send(piece, strip(side, r, f, c), x_s.at[c], x_r.at[c], {"tp": across}).start()
+    depart(1)
     landing = qt.at[side, at(r * half, half, half)]
     send(landing, landing, q_s, q_r, mate).start()
 
@@ -718,15 +721,29 @@
     survey(gb, 0, width, False, width)
     gb[width:, :width] = gb[:width, width:].T
     inverse_b, scale_b = scales()
-    both = lambda: arrived(qt.at[side, at(other * half, half, half)], q_r)
-    done = product(4, small, gb, gb, b1, poly_one(inverse_b), both)
-    done = product(5, small, gb, b1, b2, times(inverse_b), done)
+    def square(lhs, rhs, out, finish):
+        def step(n, carry):
+            i, j = n // 2, (n + 1) // 2
+            rows, cols = at(i * width, width, width), at(j * width, width, width)
+            acc = jnp.dot(lhs[rows, :small], rhs[:small, cols], preferred_element_type=F32)
+            value = finish(acc, lhs, rows, cols, (j - i) * width).astype(BF16)
+            out[rows, cols] = value
+
+            @pl.when(i != j)
+            def _():
+                out[cols, rows] = value.T
+
+            return carry
+
+        lax.fori_loop(0, 3, step, 0)
+
+    square(gb, gb, b1, poly_one(inverse_b))
+    square(gb, b1, b2, times(inverse_b))
     travel(0, 0)
-    done = product(6, small, b2, b1, b0, plain, done)
+    square(b2, b1, b0, plain)
     travel(0, 1)
-    done = product(7, small, b0, b0, b2, poly_two, done)
+    square(b0, b0, b2, poly_two)
     travel(1, 0)
-    done()
     c2[:thin, :small] = b2[at(t * thin, thin, thin), :small]
 
     def tasks_b(n):
@@ -734,6 +751,8 @@
             travel(1, 1)
         if n == 3:
             travel(2, 0)
+        if n == 5:
+            travel(2, 1)
 
     factor(
         thin, t * thin, 0, view(b0, 0, small), view(b1, 0, small), view(b2, 0, small),
@@ -776,10 +795,10 @@
         local(weights[m], speed[m], 12 + m).wait()
     update(2, lambda rows: sb[rows, :], lambda: qtb[...], rate_b, put_small, low, CHUNK)
     local(velb, bu, 17).start()
-    travel(2, 1)
     ring_in(0, ntp - 1)
     ring_in(1, 1)
     ring_in(1 - side, 2)
+    arrived(qt.at[side, at(other * half, half, half)], q_r)
     finish_big(side)
     for d in range(3, nfs):
         travel(d, 0)
@@ -861,7 +880,7 @@
     scratch += [dma((18,)), dma((3,)), dma((3,)), dma((3, ntp)), dma((3, ntp))]
     scratch += [slots] * 2 + [dma((5 + blocks, 4))] * 5
     scratch += [dma((5, 4, 2)), dma((10, 4)), dma((10, 4)), dma((10, 4)), dma((blocks,)), dma((blocks,))]
-    scratch += [dma((8, 5))] * 2 + [dma, dma, dma((2,)), dma((2,))] + [dma((2, 2 * nfs))] * 4
+    scratch += [dma((4, 5))] * 2 + [dma, dma, dma((2,)), dma((2,))] + [dma((2, 2 * nfs))] * 4
     outs = []
     for i in range(3):
         outs += [jax.ShapeDtypeStruct(args[3 * i + 1].shape, F32)] * 2

time: 175 us -> 174 us (level)
  no operation moved by 1% of the time
where the time goes in v4:
time: 174 us
  Pallas kernels  173 us (99%)
    pallas_call x1, Pallas kernels, local_part(): pl.pallas_call(functools.partial(kernel, nfs, ntp), out_shape=tuple(outs)...  168 us
    pallas_call x1, Pallas kernels, local_part(): pl.pallas_call(hand_over, out_shape=tuple(outs), in_specs=[pl.BlockSpec(m...  5.32 us

profile of v4, /device:TPU:7, one launch (start us, length us, event | category | flops | bytes accessed | tf_op | source)
XLA Modules:
  0.0 173.9 jit_solution(4790269572399475728)
XLA Ops:
  0.6 167.7 %orthogonal.1 = (f32[704,512]{1,0:T(8,128)}, f32[704,512]{1,0:T(8,128)}, f32[704,512]{1,0:T(8,128)}, f32[704,512]{1,0:T(8,128)}, f32[256,256]{1,0:T(8,128)}, /*index=5*/f32[256,256]{1,0:T(8,128)}) custom-call(f32[1,1408,512]{2,1,0:T(8,128)} %refs_0_.1, f32[704,512]{1,0:T(8,128)} %refs_1_.1, f32[704,512]{1,0:T(8,128)} %refs_2_.1, f32[1,1408,512]{2,1,0:T(8,128)} %refs_3_.1, ...), custom_call_target="tpu_custom_call" | custom-call | tf_op jit(solution)/shard_map/orthogonal/pallas_call | solution.py:887
  168.4 5.3 %hand_over.1 = (f32[704,512]{1,0:T(8,128)}, f32[704,512]{1,0:T(8,128)}, f32[704,512]{1,0:T(8,128)}, f32[704,512]{1,0:T(8,128)}, f32[256,256]{1,0:T(8,128)}, /*index=5*/f32[256,256]{1,0:T(8,128)}) custom-call(f32[704,512]{1,0:T(8,128)} %get-tuple-element.12.refs_0_, f32[704,512]{1,0:T(8,128)} %get-tuple-element.13.refs_1_, ...), custom_call_target="tpu_custom_call" | custom-call | tf_op jit(solution)/shard_map/hand_over/pallas_call | solution.py:899
